TPU v7x, 32 devices: a whole 2x2x4 slice. The times are simulated.
32 devices in a mesh: sp: 8 (over z, core), tp: 4 (over y, x).
Axes of the slice: x: 2, y: 2, z: 4, core: 2. Of those that a mesh axis runs over, the one named last changes fastest.
Arguments:
- resid: bfloat16 [2048, 2048], P('sp'), may hold values from -18 to 18
- narrow_head_input: bfloat16 [2048, 1024], P('sp', 'tp'), may hold values from -6 to 6
- wide_head_input: bfloat16 [2048, 2048], P('sp', 'tp'), may hold values from -6 to 6
- key_group_input: bfloat16 [2048, 512], P('sp'), may hold values from -6 to 6
- query_group_input: bfloat16 [2048, 512], P('sp'), may hold values from -6 to 6
- narrow_output_gate: bfloat16 [2048, 1024], P('sp', 'tp'), may hold values from -6 to 6
- wide_output_gate: bfloat16 [2048, 2048], P('sp', 'tp'), may hold values from -6 to 6
- step_input_rows: bfloat16 [2048, 2, 16], P('sp', None, 'tp'), may hold values from -4 to 4
- head_decay_logarithm: float32 [2, 16], P(None, 'tp'), may hold values from -14 to -2
- position_log_decay: float32 [2048, 2, 16], P('sp', None, 'tp'), may hold values from -1.4 to 0
- direct_input_weight: float32 [2, 16], P(None, 'tp'), may hold values from 0.5 to 2
- narrow_conv_taps: float32 [4, 1024], P(None, 'tp'), may hold values from -3 to 3
- wide_conv_taps: float32 [4, 2048], P(None, 'tp'), may hold values from -3 to 3
- key_conv_taps: float32 [4, 512], replicated, may hold values from -3 to 3
- query_conv_taps: float32 [4, 512], replicated, may hold values from -3 to 3
- narrow_norm_gain: float32 [1024], P('tp'), may hold values from 0.1 to 1.9
- wide_norm_gain: float32 [2048], P('tp'), may hold values from 0.1 to 1.9
- narrow_output_rows: bfloat16 [1024, 2048], P('tp'), may hold values from -0.109375 to 0.109375
- wide_output_rows: bfloat16 [2048, 2048], P('tp'), may hold values from -0.109375 to 0.109375
- feedforward_norm_gain: float32 [2048], replicated, may hold values from 0.1 to 1.9
- routes: int32 [2048, 3], P('sp'), may hold values from 0 to 7, all different within a row; in each aligned block of 256 rows (0 to 255, 256 to 511, ...) at most 128 rows name the same one
- routing_weight_values: float32 [2048, 3], P('sp'), may hold values from 0.1 to 1
- expert_gate_matrix: bfloat16 [8, 2048, 2048], P('sp', None, 'tp'), may hold values from -1 to 1
- expert_up_matrix: bfloat16 [8, 2048, 2048], P('sp', None, 'tp'), may hold values from -1 to 1
- expert_down_matrix: bfloat16 [8, 2048, 2048], P('sp', 'tp'), may hold values from -0.015625 to 0.015625
Outputs:
- layer_out: bfloat16 [2048, 2048], P('sp', 'tp')
Inputs may be any that keep to these rules, and one draw needn't show every extreme that they name: `routes`: each token names 3 different experts. Among the tokens of one index of sp (aligned blocks of 256 rows) no expert is named by more than 128 of them, and in some blocks one is named by exactly 128.
All inputs are finite; a program needn't handle non-finite values.
Results may differ from a plain program's by a relative error of at most 0.015.
Values may be sent and summed in bfloat16 or wider, within the bound.
A program may use at most 64 MiB of HBM per device.

v0:
```python
import functools

import jax
import jax.numpy as jnp
from jax import lax
from jax.experimental import pallas as pl
from jax.experimental.pallas import tpu as pltpu
from jax.sharding import PartitionSpec as P

HEADS = 16
NARROW_HEAD_DIM = 64
WIDE_HEAD_DIM = 128
GROUPS = 4
BLOCK = 128


NORM_EPS = 1e-06
CLAMP_LIMIT = 7.0
SIGMOID_SCALE = 1.702
FULL_PRECISION = lax.Precision.HIGHEST


def passed_along(block, axis, distance):
    devices = range(lax.axis_size(axis))
    route = [(i - distance, i) for i in devices if i - distance in devices]
    return lax.ppermute(block, axis, route)


def entering(narrow_parts, wide_parts, axis):
    place = lax.axis_index(axis)
    narrow_states, wide_states = narrow_parts[2], wide_parts[2]
    heads, state_size, narrow_size = narrow_states.shape
    totals = jnp.stack([narrow_parts[3], wide_parts[3]], axis=1)
    total_rows = jnp.broadcast_to(
        jnp.repeat(totals, 4, axis=1)[:, :, None], (heads, 8, narrow_size)
    )
    narrow_packed = jnp.concatenate([narrow_states, total_rows], axis=1).astype(jnp.bfloat16)
    narrow_all, wide_all = lax.all_gather((narrow_packed, wide_states.astype(jnp.bfloat16)), axis)
    count = narrow_all.shape[0]
    earlier = jnp.arange(count) < place
    between = jnp.logical_and(
        jnp.arange(count)[:, None] < jnp.arange(count)[None, :], earlier[None, :]
    )

    def carry(states, row):
        decay = narrow_all[:, :, state_size + row, 0].astype(jnp.float32)
        gap = jnp.sum(jnp.where(between[:, :, None], decay[None], 0.0), axis=1)
        factor = jnp.where(earlier[:, None], jnp.exp(gap), 0.0)
        return jnp.sum(factor[:, :, None, None] * states.astype(jnp.float32), axis=0)

    return carry(narrow_all[:, :, :state_size], 0), carry(wide_all, 4)


def conv_with_rim(values, rim_rows, weight):
    length = values.shape[0]
    padded = jnp.concatenate([rim_rows, values], axis=0).astype(jnp.float32)
    accumulated = jnp.zeros((length, values.shape[1]), jnp.float32)
    for tap_index in range(weight.shape[0]):
        accumulated = accumulated + weight[tap_index] * padded[tap_index : tap_index + length]
    return jax.nn.silu(accumulated)


def local_head(values, step_logarithm, key_head_rows, query_head_rows, block_len):
    block_count = values.shape[0] // block_len
    values = values.reshape(block_count, block_len, -1)
    step_logarithm = step_logarithm.reshape(block_count, block_len)
    key_head_rows = key_head_rows.reshape(block_count, block_len, -1)
    query_head_rows = query_head_rows.reshape(block_count, block_len, -1)
    cum_decay = jnp.cumsum(step_logarithm, axis=1)
    causal_mask = jnp.arange(block_len)[:, None] >= jnp.arange(block_len)[None, :]
    decay_gaps = jnp.where(causal_mask[None], cum_decay[:, :, None] - cum_decay[:, None, :], -1e30)
    scores = jnp.einsum(
        "bln,bsn->bls", query_head_rows, key_head_rows, precision=FULL_PRECISION
    ) * jnp.exp(decay_gaps)
    inside = jnp.einsum("bls,bsp->blp", scores, values, precision=FULL_PRECISION)
    tail_decay = jnp.exp(cum_decay[:, -1:] - cum_decay)
    states = jnp.einsum(
        "bln,blp->bnp", key_head_rows * tail_decay[..., None], values, precision=FULL_PRECISION
    )
    totals = cum_decay[:, -1]

    def walk(running, member):
        return (jnp.exp(member[1]) * running + member[0], running)

    closing, entering = lax.scan(walk, jnp.zeros(states.shape[1:], jnp.float32), (states, totals))
    before = jnp.cumsum(totals) - totals
    return (inside, entering, closing, jnp.sum(totals), before, cum_decay, query_head_rows)


def finish_head(inside, entering, before, cum_decay, query_blocks, carried):
    starting = entering + jnp.exp(before)[:, None, None] * carried[None]
    readout = jnp.einsum(
        "bln,bnp->blp",
        query_blocks * jnp.exp(cum_decay)[..., None],
        starting,
        precision=FULL_PRECISION,
    )
    return (inside + readout).reshape(-1, inside.shape[-1])


def group_out(scanned, mixed_input_rows, direct_input_term, gate_input_rows, norm_gain_vector):
    length, head_count, head_dimension = mixed_input_rows.shape
    gated = jax.nn.silu(gate_input_rows.astype(jnp.float32)).reshape(
        length, head_count, head_dimension
    )
    result = (scanned + direct_input_term[None, :, None] * mixed_input_rows) * gated
    result = result * lax.rsqrt(jnp.mean(result * result, axis=-1, keepdims=True) + NORM_EPS)
    return (result.reshape(length, head_count * head_dimension) * norm_gain_vector).astype(
        jnp.bfloat16
    )


def head_pieces_list(
    mixed_input_rows,
    step_length_values,
    decay_vector,
    position_decay_rows,
    key_head_rows,
    query_head_rows,
):
    step_logarithm = -jnp.exp(decay_vector)[None, :] * step_length_values + position_decay_rows
    values = mixed_input_rows * step_length_values[..., None]
    walker = functools.partial(local_head, block_len=BLOCK)
    return jax.vmap(walker, in_axes=(1, 1, None, None))(
        values, step_logarithm, key_head_rows, query_head_rows
    )


def finish_group(parts, carried_states):
    return jax.vmap(finish_head, in_axes=(0, 0, 0, 0, 0, 0), out_axes=1)(
        parts[0], parts[1], parts[4], parts[5], parts[6], carried_states
    )


def ring_map(index, count):
    side = int(round(count**0.5))
    if side * side != count:
        return index
    row = index // side
    column = index % side
    return row * side + column + (row % 2) * (side - 1 - 2 * column)


def tail_kernel(
    shards,
    experts,
    narrow_ref,
    wide_ref,
    narrow_rows_ref,
    wide_rows_ref,
    resid_ref,
    gain_ref,
    rank_ref,
    weight_ref,
    gate_hbm,
    up_hbm,
    down_hbm,
    out_ref,
    gate_v,
    up_v,
    down_v,
    share_out,
    share_in,
    square_out,
    square_in,
    hidden,
    normed,
    dispatch_out,
    tokens,
    partial,
    sums,
    done_out,
    done_in,
    load_sem,
    share_send,
    share_recv,
    square_send,
    square_recv,
    dispatch_send,
    dispatch_recv,
    gather_send,
    gather_recv,
    sum_send,
    sum_recv,
    done_send,
    done_recv,
):
    me_s = lax.axis_index("sp")
    me_t = lax.axis_index("tp")
    length, width = resid_ref.shape
    capacity = done_in.shape[1]
    groups = tokens.shape[1]
    sources = experts // groups
    half = tokens.shape[2] // 2
    place = ring_map(me_t, shards)
    after = ring_map((place + 1) % shards, shards)
    before = ring_map((place + shards - 1) % shards, shards)

    def remote(src, dst, send, recv, where):
        return pltpu.make_async_remote_copy(
            src_ref=src,
            dst_ref=dst,
            send_sem=send,
            recv_sem=recv,
            device_id=where,
            device_id_type=pl.DeviceIdType.MESH,
        )

    loads = [
        pltpu.make_async_copy(h, v, load_sem.at[i])
        for i, (h, v) in enumerate(((gate_hbm, gate_v), (up_hbm, up_v), (down_hbm, down_v)))
    ]
    for load in loads:
        load.start()

    barrier = pltpu.get_barrier_semaphore()

    def greet_tp(d, c):
        pl.semaphore_signal(
            barrier,
            inc=1,
            device_id=(me_s, (me_t + d) % shards),
            device_id_type=pl.DeviceIdType.MESH,
        )
        return c

    def greet_sp(d, c):
        pl.semaphore_signal(
            barrier,
            inc=1,
            device_id=((me_s + d) % experts, me_t),
            device_id_type=pl.DeviceIdType.MESH,
        )
        return c

    lax.fori_loop(1, shards, greet_tp, 0)
    lax.fori_loop(1, experts, greet_sp, 0)
    pl.semaphore_wait(barrier, shards + experts - 2)

    def project(block):
        columns = pl.ds(pl.multiple_of(block * width, 128), width)
        return (
            jnp.dot(
                narrow_ref[...], narrow_rows_ref[:, columns], preferred_element_type=jnp.float32
            )
            + jnp.dot(wide_ref[...], wide_rows_ref[:, columns], preferred_element_type=jnp.float32)
        ).astype(jnp.bfloat16)

    def share_copy(d):
        return remote(
            share_out.at[d],
            share_in.at[d],
            share_send.at[d],
            share_recv.at[d],
            (me_s, (me_t + d) % shards),
        )

    def send_share(d, c):
        share_out[d] = project((me_t + d) % shards)
        share_copy(d).start()
        return c

    lax.fori_loop(1, shards, send_share, 0)
    hidden[...] = resid_ref[...].astype(jnp.float32) + project(me_t).astype(jnp.float32)

    def take_share(d, c):
        share_copy(d).wait_recv()
        hidden[...] += share_in[d].astype(jnp.float32)
        return c

    lax.fori_loop(1, shards, take_share, 0)
    state = hidden[...]
    own_square = jnp.sum(state * state, axis=1, keepdims=True)
    square_rows = jnp.transpose(jnp.broadcast_to(own_square, (length, 128)))
    square_out[...] = square_rows[:8]

    def square_copy(d):
        return remote(
            square_out,
            square_in.at[d],
            square_send.at[d],
            square_recv.at[d],
            (me_s, (me_t + d) % shards),
        )

    def send_square(d, c):
        square_copy(d).start()
        return c

    lax.fori_loop(1, shards, send_square, 0)

    def take_square(d, total):
        square_copy(d).wait_recv()
        return total + square_in[d]

    total = lax.fori_loop(1, shards, take_square, square_rows[:8])
    scale_row = lax.rsqrt(total[:1] / (shards * width) + NORM_EPS)
    scale = jnp.transpose(jnp.broadcast_to(scale_row, (128, length)))[:, :1]
    normed[...] = (hidden[...] * scale * gain_ref[...]).astype(jnp.bfloat16)

    slots = lax.broadcasted_iota(jnp.int32, (capacity, length), 0)

    def pick(d):
        chooser = jnp.where(slots == rank_ref[d], 1.0, 0.0).astype(jnp.bfloat16)
        return jnp.dot(chooser, normed[...], preferred_element_type=jnp.float32).astype(
            jnp.bfloat16
        )

    def dispatch_copy(d):
        return remote(
            dispatch_out.at[d],
            tokens.at[me_t, d // sources, pl.ds((d % sources) * capacity, capacity)],
            dispatch_send.at[d],
            dispatch_recv.at[d],
            ((me_s + d) % experts, me_t),
        )

    def send_dispatch(d, c):
        dispatch_out[d] = pick(d)
        dispatch_copy(d).start()
        return c

    tokens[me_t, 0, :capacity] = pick(0)
    lax.fori_loop(1, experts, send_dispatch, 0)

    def gather_copy(way, hop, d):
        step_back = hop - 1 if way else shards - hop + 1
        block = ring_map((place + step_back) % shards, shards)
        part = tokens.at[block, d, pl.ds(way * half, half)]
        return remote(
            part,
            part,
            gather_send.at[way, hop, d],
            gather_recv.at[way, hop, d],
            (me_s, before if way else after),
        )

    def sum_block(way, hop):
        if way:
            return ring_map((place + hop) % shards, shards)
        return ring_map((place + shards - hop) % shards, shards)

    def sum_copy(way, hop, d):
        source = sums.at[way, hop - 1, d]
        return remote(
            source,
            sums.at[way, hop, d],
            sum_send.at[way, hop, d],
            sum_recv.at[way, hop, d],
            (me_s, before if way else after),
        )

    def done_copy(d):
        return remote(
            done_out.at[d // sources, pl.ds((d % sources) * capacity, capacity)],
            done_in.at[d],
            done_send.at[d],
            done_recv.at[d],
            ((me_s + experts - d) % experts, me_t),
        )

    def expert(d):
        gate = jnp.zeros((2 * half, gate_v.shape[1]), jnp.float32)
        up = jnp.zeros((2 * half, gate_v.shape[1]), jnp.float32)
        for j in range(shards):
            rows = pl.ds(j * width, width)
            piece = tokens[j, d]
            gate += jnp.dot(piece, gate_v[rows, :], preferred_element_type=jnp.float32)
            up += jnp.dot(piece, up_v[rows, :], preferred_element_type=jnp.float32)
        clamped = jnp.minimum(gate, CLAMP_LIMIT)
        act = (
            (jnp.clip(up, -CLAMP_LIMIT, CLAMP_LIMIT) + 1.0)
            * clamped
            * jax.nn.sigmoid(SIGMOID_SCALE * clamped)
        ).astype(jnp.bfloat16)
        for j in range(shards):
            partial[j, d] = jnp.dot(
                act, down_v[:, j * width : (j + 1) * width], preferred_element_type=jnp.float32
            ).astype(jnp.bfloat16)

    last = shards - 1

    def step(i, c):
        @pl.when(i < groups)
        def _():
            def arrive(d, c):
                @pl.when(d > 0)
                def _():
                    dispatch_copy(d).wait_recv()

                return c

            lax.fori_loop(i * sources, (i + 1) * sources, arrive, 0)

            for way in range(2):
                gather_copy(way, 1, i).start()

        def gather_hop(hop, c):
            d = i - hop + 1

            @pl.when(jnp.logical_and(d >= 0, d < groups))
            def _():
                for way in range(2):
                    gather_copy(way, hop - 1, d).wait_recv()
                    gather_copy(way, hop, d).start()

            return c

        lax.fori_loop(2, shards, gather_hop, 0)

        def sum_hop(hop, c):
            d = i - last - hop + 1

            @pl.when(jnp.logical_and(d >= 0, d < groups))
            def _():
                for way in range(2):
                    sum_copy(way, hop - 1, d).wait_recv()
                    sums[way, hop - 1, d] = (
                        sums[way, hop - 1, d].astype(jnp.float32)
                        + partial[sum_block(way, hop), d, way * half : (way + 1) * half].astype(
                            jnp.float32
                        )
                    ).astype(jnp.bfloat16)
                    sum_copy(way, hop, d).start()

            return c

        lax.fori_loop(2, shards, sum_hop, 0)
        finished = i - 2 * last

        @pl.when(finished >= 0)
        def _():
            for way in range(2):
                sum_copy(way, last, finished).wait_recv()
                done_out[finished, way * half : (way + 1) * half] = (
                    sums[way, last, finished].astype(jnp.float32)
                    + partial[me_t, finished, way * half : (way + 1) * half].astype(jnp.float32)
                ).astype(jnp.bfloat16)

            def leave(d, c):
                @pl.when(d > 0)
                def _():
                    done_copy(d).start()

                return c

            lax.fori_loop(finished * sources, (finished + 1) * sources, leave, 0)

        ready = i - last

        @pl.when(jnp.logical_and(ready >= 0, ready < groups))
        def _():
            for way in range(2):
                gather_copy(way, last, ready).wait_recv()

            @pl.when(ready == 0)
            def _():
                for load in loads:
                    load.wait()

            expert(ready)
            for way in range(2):
                sums[way, 0, ready] = partial[
                    sum_block(way, 1), ready, way * half : (way + 1) * half
                ]
                sum_copy(way, 1, ready).start()

        return c

    lax.fori_loop(0, groups + 2 * last, step, 0)

    def combine(d, rows):
        weights = jnp.where(slots == rank_ref[d], weight_ref[d], 0.0)
        high = weights.astype(jnp.bfloat16)
        low = (weights - high.astype(jnp.float32)).astype(jnp.bfloat16)
        over_slots = (((0,), (0,)), ((), ()))
        return lax.dot_general(
            high, rows, over_slots, preferred_element_type=jnp.float32
        ) + lax.dot_general(low, rows, over_slots, preferred_element_type=jnp.float32)

    hidden[...] += combine(0, done_out[0, :capacity])

    def take_done(d, c):
        done_copy(d).wait_recv()
        hidden[...] += combine(d, done_in[d])
        return c

    lax.fori_loop(1, experts, take_done, 0)
    out_ref[...] = hidden[...].astype(jnp.bfloat16)

    def finish_tp(d, c):
        share_copy(d).wait_send()
        square_copy(d).wait_send()
        return c

    lax.fori_loop(1, shards, finish_tp, 0)

    def finish_sp(d, c):
        dispatch_copy(d).wait_send()
        done_copy(d).wait_send()
        return c

    lax.fori_loop(1, experts, finish_sp, 0)

    def finish_chunk(d, c):
        def finish_hop(hop, c):
            for way in range(2):
                gather_copy(way, hop, d).wait_send()
                sum_copy(way, hop, d).wait_send()
            return c

        return lax.fori_loop(1, shards, finish_hop, c)

    lax.fori_loop(0, groups, finish_chunk, 0)


def tail_call(*operands):
    *arrays, capacity = operands
    shards, experts = lax.axis_size("tp"), lax.axis_size("sp")
    length, width = arrays[4].shape
    gate, up, down = arrays[8:]
    sources = max(1, min(experts, 128 // capacity))
    groups = experts // sources
    rows = sources * capacity
    bf16, f32 = jnp.bfloat16, jnp.float32
    vmem = pl.BlockSpec(memory_space=pltpu.VMEM)
    dma = pltpu.SemaphoreType.DMA
    return pl.pallas_call(
        functools.partial(tail_kernel, shards, experts),
        out_shape=jax.ShapeDtypeStruct((length, width), bf16),
        in_specs=[vmem] * 8 + [pl.BlockSpec(memory_space=pl.ANY)] * 3,
        out_specs=vmem,
        scratch_shapes=[
            pltpu.VMEM(gate.shape, bf16),
            pltpu.VMEM(up.shape, bf16),
            pltpu.VMEM(down.shape, bf16),
            pltpu.VMEM((shards, length, width), bf16),
            pltpu.VMEM((shards, length, width), bf16),
            pltpu.VMEM((8, length), f32),
            pltpu.VMEM((shards, 8, length), f32),
            pltpu.VMEM((length, width), f32),
            pltpu.VMEM((length, width), bf16),
            pltpu.VMEM((experts, capacity, width), bf16),
            pltpu.VMEM((shards, groups, rows, width), bf16),
            pltpu.VMEM((shards, groups, rows, width), bf16),
            pltpu.VMEM((2, shards, groups, rows // 2, width), bf16),
            pltpu.VMEM((groups, rows, width), bf16),
            pltpu.VMEM((experts, capacity, width), bf16),
            dma((3,)),
            dma((shards,)),
            dma((shards,)),
            dma((shards,)),
            dma((shards,)),
            dma((experts,)),
            dma((experts,)),
            dma((2, shards, groups)),
            dma((2, shards, groups)),
            dma((2, shards, groups)),
            dma((2, shards, groups)),
            dma((experts,)),
            dma((experts,)),
        ],
        compiler_params=pltpu.CompilerParams(
            collective_id=0, has_side_effects=True, vmem_limit_bytes=56 * 1024 * 1024
        ),
    )(*arrays)


def local(
    resid,
    narrow_head_input,
    wide_head_input,
    key_group_input,
    query_group_input,
    narrow_output_gate,
    wide_output_gate,
    step_input_rows,
    head_decay_logarithm,
    position_log_decay,
    direct_input_weight,
    narrow_conv_taps,
    wide_conv_taps,
    key_conv_taps,
    query_conv_taps,
    narrow_norm_gain,
    wide_norm_gain,
    narrow_output_rows,
    wide_output_rows,
    feedforward_norm_gain,
    routes,
    routing_weight_values,
    expert_gate_matrix,
    expert_up_matrix,
    expert_down_matrix,
):
    length = resid.shape[0]
    head_count = narrow_head_input.shape[1] // NARROW_HEAD_DIM
    rim_len = narrow_conv_taps.shape[0] - 1
    first_head = lax.axis_index("tp") * head_count
    state_size = key_group_input.shape[1] // GROUPS
    group_column = first_head // (HEADS // GROUPS) * state_size

    def own_group(table):
        return lax.dynamic_slice_in_dim(table, group_column, state_size, 1)

    streams = (
        narrow_head_input,
        wide_head_input,
        own_group(key_group_input),
        own_group(query_group_input),
    )
    rims = passed_along(
        jnp.concatenate([stream[length - rim_len :] for stream in streams], axis=1), "sp", 1
    )
    edges = [0]
    for stream in streams:
        edges.append(edges[-1] + stream.shape[1])
    rim_rows = [rims[:, low:high] for low, high in zip(edges[:-1], edges[1:])]
    narrow_head_mix = conv_with_rim(narrow_head_input, rim_rows[0], narrow_conv_taps).reshape(
        length, head_count, NARROW_HEAD_DIM
    )
    wide_head_mix = conv_with_rim(wide_head_input, rim_rows[1], wide_conv_taps).reshape(
        length, head_count, WIDE_HEAD_DIM
    )
    key_head_rows = conv_with_rim(streams[2], rim_rows[2], own_group(key_conv_taps))
    query_head_rows = conv_with_rim(streams[3], rim_rows[3], own_group(query_conv_taps))
    step_length_values = jax.nn.softplus(step_input_rows.astype(jnp.float32))
    narrow_parts = head_pieces_list(
        narrow_head_mix,
        step_length_values[:, 0],
        head_decay_logarithm[0],
        position_log_decay[:, 0],
        key_head_rows,
        query_head_rows,
    )
    wide_parts = head_pieces_list(
        wide_head_mix,
        step_length_values[:, 1],
        head_decay_logarithm[1],
        position_log_decay[:, 1],
        key_head_rows,
        query_head_rows,
    )
    narrow_carry, wide_carry = entering(narrow_parts, wide_parts, "sp")
    narrow_head_output = group_out(
        finish_group(narrow_parts, narrow_carry),
        narrow_head_mix,
        direct_input_weight[0],
        narrow_output_gate,
        narrow_norm_gain,
    )
    wide_head_output = group_out(
        finish_group(wide_parts, wide_carry),
        wide_head_mix,
        direct_input_weight[1],
        wide_output_gate,
        wide_norm_gain,
    )
    experts = lax.axis_size("sp")
    shards = lax.axis_size("tp")
    picks = routes.shape[1]
    capacity = 4 * length * picks // (3 * experts)
    width = resid.shape[1] // shards
    tp_index = lax.axis_index("tp")
    expert_order = (lax.axis_index("sp") + jnp.arange(experts, dtype=jnp.int32)) % experts
    hits = routes[None] == expert_order[:, None, None]
    member = jnp.any(hits, axis=2)
    weight_rows = jnp.sum(jnp.where(hits, routing_weight_values[None], 0.0), axis=2)
    earlier = (jnp.arange(length)[:, None] < jnp.arange(length)[None, :]).astype(jnp.bfloat16)
    ranks = jnp.dot(
        member.astype(jnp.bfloat16), earlier, preferred_element_type=jnp.float32
    ).astype(jnp.int32)
    rank_rows = jnp.where(member, ranks, -1)
    resid_own = lax.dynamic_slice_in_dim(resid, tp_index * width, width, 1)
    gain_own = lax.dynamic_slice_in_dim(feedforward_norm_gain, tp_index * width, width, 0)
    return tail_call(
        narrow_head_output,
        wide_head_output,
        narrow_output_rows,
        wide_output_rows,
        resid_own,
        gain_own[None, :],
        rank_rows[:, None, :],
        weight_rows[:, None, :],
        expert_gate_matrix[0],
        expert_up_matrix[0],
        expert_down_matrix[0],
        capacity,
    )


def solution(mesh):
    return jax.shard_map(
        local,
        mesh=mesh,
        in_specs=(
            P("sp", None),
            P("sp", "tp"),
            P("sp", "tp"),
            P("sp", None),
            P("sp", None),
            P("sp", "tp"),
            P("sp", "tp"),
            P("sp", None, "tp"),
            P(None, "tp"),
            P("sp", None, "tp"),
            P(None, "tp"),
            P(None, "tp"),
            P(None, "tp"),
            P(),
            P(),
            P("tp"),
            P("tp"),
            P("tp", None),
            P("tp", None),
            P(),
            P("sp", None),
            P("sp", None),
            P("sp", None, "tp"),
            P("sp", None, "tp"),
            P("sp", "tp", None),
        ),
        out_specs=P("sp", "tp"),
        check_vma=False,
    )
```

profile of v0, /device:TPU:0, one launch (start us, length us, event | category | flops | bytes accessed | tf_op | source)
XLA Modules:
  0.0 214.1 jit_solution(10420105761537303697)
XLA Ops:
  6.6 0.9 dynamic-slice.1
  9.8 2.4 %collective-permute-start = (bf16[3,1024]{0,1:T(8,128)(2,1)S(1)}, bf16[3,1024]{0,1:T(8,128)(2,1)S(1)}, u32[]{:S(2)}, u32[]{:S(2)}) collective-permute-start(bf16[3,1024]{0,1:T(8,128)(2,1)S(1)} %copy.183), channel_id=1, source_target_pairs={{0,4},{4,8},{8,12},{12,16},{16,20},{20,24},{24,28},{1,5},{5,9},{9,... | collective-permute-start | bytes 18440 | tf_op jit(solution)/shard_map/ppermute | solution.py:26
  12.2 1.5 constant_dynamic-slice_fusion.5
  16.0 1.2 reduce_window_sum.34
  17.3 1.2 reduce_window_sum.36
  19.7 1.3 slice_bitcast_fusion.2
  24.4 1.1 convert_multiply_fusion.1
  25.5 0.9 fusion.84
  30.7 1.0 reshape.267
  31.9 1.4 dynamic_slice.38
  36.7 1.1 convolution_bitcast_fusion.1
  37.8 2.0 while.26
  39.9 18.4 %all_gather.10 = bf16[8,4,136,64]{2,3,1,0:T(8,128)(2,1)S(1)} all-gather(bf16[1,4,136,64]{2,3,1,0:T(8,128)(2,1)S(1)} %pad_maximum_fusion), channel_id=1, replica_groups=mesh['sp'=8,'tp'=4] {'sp'}, dimensions={0}, use_global_device_ids=true | all-gather | bytes 626688 | tf_op jit(solution)/shard_map/all_gather | solution.py:38
  60.3 0.9 slice.235
  62.9 3.0 %while.27 = (s32[]{:T(128)}, f32[4,128,128]{2,1,0:T(8,128)S(1)}, f32[2,4,128,128]{3,2,1,0:T(8,128)}, f32[2,4]{1,0:T(2,128)}, f32[2,4,128,128]{3,2,0,1:T(8,128)S(1)}, /*index=5*/s32[]{:T(128)}, s32[]{:T(128)}) while((s32[]{:T(128)}, f32[4,128,128]{2,1,0:T(8,128)S(1)}, f32[2,4,128,128]{3,2,1,0:T(8,128)}, f32[2,4]{1,0:T(2,128)}, ...), condition=%wide.region_11.12_spmd.clone, body=%wide.region_10.11_spmd.clone.sunk | while | flops 262147 | bytes 1310876 | solution.py:85
  66.7 0.9 maximum_convert_fusion.2
  68.9 2.3 %fusion.15 = f32[4,2,128,64]{2,3,1,0:T(8,128)S(1)} fusion(f32[4,2,128]{2,1,0:T(2,128)} %get-tuple-element.203, f32[2,128,128]{2,1,0:T(8,128)S(1)} %bitcast.172, f32[2,4,128,64]{3,2,1,0:T(8,128)} %get-tuple-element.61, f32[4,128,64]{2,1,0:T(8,128)S(1)} %copy.198, f32[4,2]{0,1:T(2,128)} %subtract_exponential_fusion.3), kind=kOutput, calls=%fused_computation.38 | convolution fusion | flops 100925440 | bytes 790560 | tf_op jit(solution)/shard_map/vmap(bln,bnp->blp)/dot_general | solution.py:92
  71.3 1.2 fusion.5
  74.0 1.5 fusion.20
  75.5 13.5 %all-gather.3.cloned.1.call-done = bf16[32,128,128]{2,1,0:T(8,128)(2,1)} async-done(((bf16[4,128,128]{2,1,0:T(8,128)(2,1)}), bf16[32,128,128]{2,1,0:T(8,128)(2,1)}) %all-gather.3.cloned.1.call-update) | async-done | bytes 1048592 | tf_op jit(solution)/shard_map/all_gather | solution.py:38
  89.0 1.6 fusion.4
  90.6 1.8 convolution_add_fusion
  94.1 111.4 %shard_map.235 = bf16[256,512]{1,0:T(8,128)(2,1)} custom-call(bf16[256,256]{1,0:T(8,128)(2,1)} %multiply_convert_fusion.narrow_ref, bf16[256,512]{1,0:T(8,128)(2,1)} %fusion.10.wide_ref, bf16[256,2048]{1,0:T(8,128)(2,1)} %narrow_rows_ref.1, bf16[512,2048]{1,0:T(8,128)(2,1)} %wide_rows_ref.1, bf16[256,512]{1,0:T(8,128)(2,1)} %constant_dynamic-slice_fusion.3.resid_ref, ...), custom_call_target="tpu_custom_call" | custom-call | tf_op jit(solution)/shard_map/pallas_call | solution.py:528
  205.5 1.7 copy.271
  (165 shorter events, 30.9 us)
Async XLA Ops:
  6.5 22.2 %copy-start = (bf16[256,2048]{1,0:T(8,128)(2,1)S(1)}, bf16[256,2048]{1,0:T(8,128)(2,1)}, u32[]{:S(2)}) copy-start(bf16[256,2048]{1,0:T(8,128)(2,1)} %param.29) | copy-start | bytes 3145732
  6.5 23.0 %copy-start.10 = (bf16[256,256]{1,0:T(8,128)(2,1)S(1)}, bf16[256,256]{1,0:T(8,128)(2,1)}, u32[]{:S(2)}) copy-start(bf16[256,256]{1,0:T(8,128)(2,1)} %param.30) | copy-start | bytes 393220
  6.5 23.4 %copy-start.11 = (bf16[256,256]{1,0:T(8,128)(2,1)S(1)}, bf16[256,256]{1,0:T(8,128)(2,1)}, u32[]{:S(2)}) copy-start(bf16[256,256]{1,0:T(8,128)(2,1)} %param.34) | copy-start | bytes 393220
  6.5 82.5 %all-gather.3.cloned.1.call-start = ((), (), s32[]{:S(2)}) async-start(), calls=%async_computation | async-start | bytes 1179648 | tf_op jit(solution)/shard_map/all_gather | solution.py:38
  9.8 24.6 %collective-permute-start = (bf16[3,1024]{0,1:T(8,128)(2,1)S(1)}, bf16[3,1024]{0,1:T(8,128)(2,1)S(1)}, u32[]{:S(2)}, u32[]{:S(2)}) collective-permute-start(bf16[3,1024]{0,1:T(8,128)(2,1)S(1)} %copy.183), channel_id=1, source_target_pairs={{0,4},{4,8},{8,12},{12,16},{16,20},{20,24},{24,28},{1,5},{5,9},{9,... | collective-permute-start | bytes 18440 | tf_op jit(solution)/shard_map/ppermute | solution.py:26
  15.2 20.8 %copy-start.14 = (f32[256,4]{0,1:T(4,128)}, f32[256,4]{0,1:T(4,128)S(1)}, u32[]{:S(2)}) copy-start(f32[256,4]{0,1:T(4,128)S(1)} %get-tuple-element.194) | copy-start | bytes 12292
  19.6 10.1 %copy-start.13 = (f32[4,2,1]{0,1,2:T(2,128)}, f32[4,2,1]{0,1,2:T(2,128)S(1)}, u32[]{:S(2)}) copy-start(f32[4,2,1]{0,1,2:T(2,128)S(1)} %copy.206) | copy-start | bytes 100
  23.8 11.7 %copy-start.16 = (f32[1,256]{1,0:T(1,128)}, f32[1,256]{1,0:T(1,128)S(1)}, u32[]{:S(2)}) copy-start(f32[1,256]{1,0:T(1,128)S(1)} %get-tuple-element.207) | copy-start | bytes 3076
  23.8 11.7 %copy-start.18 = (f32[1,256]{1,0:T(1,128)}, f32[1,256]{1,0:T(1,128)S(1)}, u32[]{:S(2)}) copy-start(f32[1,256]{1,0:T(1,128)S(1)} %get-tuple-element.208) | copy-start | bytes 3076
  23.8 11.7 %copy-start.20 = (f32[1,256]{1,0:T(1,128)}, f32[1,256]{1,0:T(1,128)S(1)}, u32[]{:S(2)}) copy-start(f32[1,256]{1,0:T(1,128)S(1)} %get-tuple-element.209) | copy-start | bytes 3076
  23.8 11.7 %copy-start.22 = (f32[1,256]{1,0:T(1,128)}, f32[1,256]{1,0:T(1,128)S(1)}, u32[]{:S(2)}) copy-start(f32[1,256]{1,0:T(1,128)S(1)} %get-tuple-element.210) | copy-start | bytes 3076
  39.8 21.5 %copy-start.8 = (bf16[256,512]{1,0:T(8,128)(2,1)S(1)}, bf16[256,512]{1,0:T(8,128)(2,1)}, u32[]{:S(2)}) copy-start(bf16[256,512]{1,0:T(8,128)(2,1)} %param.31) | copy-start | bytes 786436
  62.9 4.6 %copy-start.4 = (f32[4,128,64]{1,2,0:T(8,128)S(1)}, f32[4,128,64]{1,2,0:T(8,128)}, u32[]{:S(2)}) copy-start(f32[4,128,64]{1,2,0:T(8,128)} %multiply_reduce_fusion) | copy-start | bytes 393220
  66.0 5.2 %copy-start.3 = (f32[256,256]{0,1:T(8,128)S(1)}, f32[256,256]{0,1:T(8,128)}, u32[]{:S(2)}) copy-start(f32[256,256]{0,1:T(8,128)} %copy-done.2) | copy-start | bytes 786436
  66.0 6.5 %copy-start.7 = (bf16[256,256]{0,1:T(8,128)(2,1)S(1)}, bf16[256,256]{0,1:T(8,128)(2,1)}, u32[]{:S(2)}) copy-start(bf16[256,256]{0,1:T(8,128)(2,1)} %copy.201) | copy-start | bytes 393220
  67.7 3.5 %copy-start.12 = (pred[128,128]{1,0:T(8,128)(4,1)S(1)}, pred[128,128]{1,0:T(8,128)(4,1)}, u32[]{:S(2)}) copy-start(pred[128,128]{1,0:T(8,128)(4,1)} %iota_compare_fusion.2) | copy-start | bytes 49156
  67.7 4.8 %copy-start.17 = (f32[1,256]{1,0:T(1,128)S(1)}, f32[1,256]{1,0:T(1,128)}, u32[]{:S(2)}) copy-start(f32[1,256]{1,0:T(1,128)} %copy-done.16) | copy-start | bytes 3076
  67.7 4.8 %copy-start.19 = (f32[1,256]{1,0:T(1,128)S(1)}, f32[1,256]{1,0:T(1,128)}, u32[]{:S(2)}) copy-start(f32[1,256]{1,0:T(1,128)} %copy-done.18) | copy-start | bytes 3076
  67.7 4.8 %copy-start.21 = (f32[1,256]{1,0:T(1,128)S(1)}, f32[1,256]{1,0:T(1,128)}, u32[]{:S(2)}) copy-start(f32[1,256]{1,0:T(1,128)} %copy-done.20) | copy-start | bytes 3076
  67.7 4.8 %copy-start.23 = (f32[1,256]{1,0:T(1,128)S(1)}, f32[1,256]{1,0:T(1,128)}, u32[]{:S(2)}) copy-start(f32[1,256]{1,0:T(1,128)} %copy-done.22) | copy-start | bytes 3076
  67.7 4.8 %copy-start.25 = (f32[4]{0:T(128)S(1)}, f32[4]{0:T(128)}, u32[]{:S(2)}) copy-start(f32[4]{0:T(128)} %get-tuple-element.220) | copy-start | bytes 52
  68.9 3.6 %copy-start.5 = (f32[2,128,128]{2,1,0:T(8,128)}, f32[2,128,128]{2,1,0:T(8,128)S(1)}, u32[]{:S(2)}) copy-start(f32[2,128,128]{2,1,0:T(8,128)S(1)} %fusion.89) | copy-start | bytes 393220
  74.0 18.4 %copy-start.27 = (f32[4]{0:T(128)S(1)}, f32[4]{0:T(128)}, u32[]{:S(2)}) copy-start(f32[4]{0:T(128)} %get-tuple-element.219) | copy-start | bytes 52
  75.5 16.9 %copy-start.1 = (f32[256,4,128]{2,1,0:T(4,128)S(1)}, f32[256,4,128]{2,1,0:T(4,128)}, u32[]{:S(2)}) copy-start(f32[256,4,128]{2,1,0:T(4,128)} %reshape.267) | copy-start | bytes 1572868
  (7 other events, 12.3 us)
Sparse Core Ops, SparseCore 0:
  66.8 22.1 all-gather.2
where the time goes:
time: 215 us; the launch traced here: 214 us
  Pallas kernels  111 us (52%)
  other arithmetic  23.1 us (11%)
  local copies, waits for them, and re-layouts  21.9 us (10%)
  blocking collectives  18.4 us (9%)
  between operations  14.1 us (7%)
  waiting for transfers between devices  13.5 us (6%)
  matrix products  9.09 us (4%)
  starting transfers between devices  2.41 us (1%)
    pallas_call x1, Pallas kernels, tail_call(): pl.pallas_call(functools.partial(tail_kernel, shards, experts), out_shape...  111 us
    all_gather x1, blocking collectives, entering(): lax.all_gather((narrow_packed, wide_states.astype(jnp.bfloat16)), axis)  18.4 us
    all_gather x1, waiting for transfers between devices, entering(): lax.all_gather((narrow_packed, wide_states.astype(jnp.bfloat16)), axis)  13.5 us
  transfers between devices with their start and end apart: 2, of which 1 were waited for; matrix products, arithmetic and copies ran while one was open for 14% of the time, Pallas kernels for 0%

commit v1 on v0

v1 whole, which is shorter than its diff:
```python
import functools

import jax
import jax.numpy as jnp
from jax import lax
from jax.experimental import pallas as pl
from jax.experimental.pallas import tpu as pltpu
from jax.sharding import PartitionSpec as P

HEADS = 16
NARROW_HEAD_DIM = 64
GROUPS = 4
LANES = 128
RIM = 16

NORM_EPS = 1e-06
CLAMP_LIMIT = 7.0
SIGMOID_SCALE = 1.702

BF16, F32 = jnp.bfloat16, jnp.float32


def sigmoid(v):
    return 0.5 * jnp.tanh(0.5 * v) + 0.5


def dot(a, b):
    return jnp.dot(a, b, preferred_element_type=F32)


def layer_kernel(
    side,
    experts,
    capacity,
    resid_hbm,
    narrow_hbm,
    wide_hbm,
    key_hbm,
    query_hbm,
    narrow_gate_hbm,
    wide_gate_hbm,
    step_hbm,
    decay_ref,
    position_hbm,
    direct_ref,
    narrow_taps_hbm,
    wide_taps_hbm,
    key_taps_hbm,
    query_taps_hbm,
    narrow_gain_hbm,
    wide_gain_hbm,
    narrow_rows_hbm,
    wide_rows_hbm,
    gain_hbm,
    routes_hbm,
    route_weights_hbm,
    gate_hbm,
    up_hbm,
    down_hbm,
    out_ref,
    wide_in,
    narrow_in,
    wide_gate_v,
    narrow_gate_v,
    step_v,
    position_v,
    narrow_taps,
    wide_taps,
    key_taps,
    query_taps,
    narrow_gain,
    wide_gain,
    head_rows_v,
    gain_v,
    routes_v,
    route_weights_v,
    resid_v,
    gate_v,
    up_v,
    down_v,
    step_rows,
    decay_rows,
    mix,
    mix_low,
    key_mix,
    query_mix,
    scores,
    base,
    gate_act,
    states,
    state_out,
    pair_in,
    chain_in,
    chain_out,
    enter,
    factor_out,
    factor_in,
    head_out,
    head_part,
    head_in1,
    head_mid,
    head_in2,
    hidden,
    hidden_low,
    chooser,
    weight_high,
    weight_low,
    dispatch_out,
    tokens,
    partial,
    sum_in1,
    sum_mid,
    sum_in2,
    done_out,
    done_in,
    load_sem,
    rim_send,
    rim_recv,
    pair_send,
    pair_recv,
    chain_send,
    chain_recv,
    relay_send,
    relay_recv,
    head_sems,
    head_sems2,
    dispatch_send,
    dispatch_recv,
    own_send,
    own_recv,
    pass_send,
    pass_recv,
    sum_sems,
    sum_sems2,
    done_send,
    done_recv,
):
    me_s = lax.axis_index("sp")
    me_t = lax.axis_index("tp")
    col = me_t % side
    row = me_t // side
    core = me_s % 2
    plane = me_s // 2
    planes = experts // 2
    length, width = resid_v.shape
    shards = side * side
    groups = tokens.shape[1]
    sources = experts // groups
    state = key_hbm.shape[1] // GROUPS
    head_count = decay_ref.shape[1]
    wide_width = wide_hbm.shape[1]
    narrow_width = narrow_hbm.shape[1]
    peers = range(1, side)
    wide_columns = wide_width // LANES
    columns = []
    for i in range(wide_columns):
        columns.append((i * LANES, LANES, (head_count + i,)))
    for i in range(-(-narrow_width // LANES)):
        size = min(LANES, narrow_width - i * LANES)
        first = i * (LANES // NARROW_HEAD_DIM)
        columns.append(
            (i * LANES, size, tuple(first + k for k in range(size // NARROW_HEAD_DIM)))
        )
    column_count = len(columns)

    def at(c, r):
        return r * side + c

    def remote(src, dst, send, recv, where):
        return pltpu.make_async_remote_copy(
            src_ref=src,
            dst_ref=dst,
            send_sem=send,
            recv_sem=recv,
            device_id=where,
            device_id_type=pl.DeviceIdType.MESH,
        )

    group_column = pl.multiple_of(me_t * head_count // (HEADS // GROUPS) * state, LANES)
    own_columns = pl.ds(pl.multiple_of(me_t * width, LANES), width)
    group_slice = pl.ds(group_column, state)
    body = pl.ds(RIM, length)
    moves = (
        (wide_hbm, wide_in.at[body, pl.ds(0, wide_width)]),
        (key_hbm.at[:, group_slice], wide_in.at[body, pl.ds(wide_width, state)]),
        (query_hbm.at[:, group_slice], wide_in.at[body, pl.ds(wide_width + state, state)]),
        (narrow_hbm, narrow_in.at[body]),
        (wide_taps_hbm, wide_taps),
        (key_taps_hbm.at[:, group_slice], key_taps),
        (query_taps_hbm.at[:, group_slice], query_taps),
        (narrow_taps_hbm, narrow_taps),
        (step_hbm, step_v),
        (position_hbm, position_v),
        (wide_gate_hbm, wide_gate_v),
        (narrow_gate_hbm, narrow_gate_v),
        (narrow_gain_hbm, narrow_gain),
        (wide_gain_hbm, wide_gain),
        (routes_hbm, routes_v),
        (route_weights_hbm, route_weights_v),
        (wide_rows_hbm, head_rows_v.at[pl.ds(0, wide_width)]),
        (narrow_rows_hbm, head_rows_v.at[pl.ds(wide_width, narrow_width)]),
        (resid_hbm.at[:, own_columns], resid_v),
        (gain_hbm, gain_v),
        (gate_hbm.at[0], gate_v),
        (up_hbm.at[0], up_v),
        (down_hbm.at[0], down_v),
    )
    loads = [pltpu.make_async_copy(s, d, load_sem.at[i]) for i, (s, d) in enumerate(moves)]
    for load in loads:
        load.start()

    barrier = pltpu.get_barrier_semaphore()

    def greet(s, t):
        pl.semaphore_signal(
            barrier, inc=1, device_id=(s, t), device_id_type=pl.DeviceIdType.MESH
        )

    def greet_sp(d, c):
        greet((me_s + d) % experts, me_t)
        return c

    lax.fori_loop(1, experts, greet_sp, 0)
    for k in peers:
        greet(me_s, at((col + k) % side, row))
        greet(me_s, at(col, (row + k) % side))
    pl.semaphore_wait(barrier, experts - 1 + 2 * (side - 1))

    for load in loads[:4]:
        load.wait()

    tail = pl.ds(length, RIM)
    head = pl.ds(0, RIM)

    def rim_copies():
        where = (me_s + 1, me_t)
        return (
            remote(wide_in.at[tail], wide_in.at[head], rim_send.at[0], rim_recv.at[0], where),
            remote(narrow_in.at[tail], narrow_in.at[head], rim_send.at[1], rim_recv.at[1], where),
        )

    @pl.when(me_s < experts - 1)
    def _():
        for copy in rim_copies():
            copy.start()

    @pl.when(me_s == 0)
    def _():
        wide_in[:RIM, :] = jnp.zeros((RIM, wide_in.shape[1]), BF16)
        narrow_in[:RIM, :] = jnp.zeros((RIM, narrow_in.shape[1]), BF16)

    for load in loads[4:10]:
        load.wait()

    def padded(v):
        if v.shape[1] == LANES:
            return v
        return jnp.concatenate([v, jnp.zeros((v.shape[0], LANES - v.shape[1]), v.dtype)], axis=1)

    def conv(source, offset, size, taps, tap_offset, first, count):
        rows = padded(source[first : first + count + RIM, offset : offset + size]).astype(F32)
        weights = padded(taps[:, tap_offset : tap_offset + size])
        total = weights[-1:] * rows
        last = taps.shape[0] - 1
        for k in range(1, last + 1):
            total = total + weights[last - k : last - k + 1] * pltpu.roll(rows, k, 0)
        total = total[RIM:]
        return total * sigmoid(total)

    def convolve(first, count):
        keep = slice(first, first + count)
        key_mix[keep, :] = conv(wide_in, wide_width, state, key_taps, 0, first, count)
        query_mix[keep, :] = conv(
            wide_in, wide_width + state, state, query_taps, 0, first, count
        ).astype(BF16)
        for j, (offset, size, _) in enumerate(columns):
            wide = j < wide_columns
            value = conv(
                wide_in if wide else narrow_in,
                offset,
                size,
                wide_taps if wide else narrow_taps,
                offset,
                first,
                count,
            )
            mix[j, keep, :] = value
            mix_low[j, keep, :] = value.astype(BF16)

    convolve(RIM, length - RIM)

    lane = lax.broadcasted_iota(jnp.int32, (1, LANES), 1)

    def spread(parts):
        if len(parts) == 1:
            return parts[0]
        return jnp.where(lane < NARROW_HEAD_DIM, parts[0], parts[1])

    step_rows[...] = jnp.ones(step_rows.shape, F32)
    decay_rows[...] = jnp.zeros(decay_rows.shape, F32)
    head_index = lax.broadcasted_iota(jnp.int32, (head_count, length), 0)
    for g in range(2):
        raw = step_v[g].astype(F32)
        soft = jnp.maximum(raw, 0.0) + jnp.log(1.0 + jnp.exp(-jnp.abs(raw)))
        rate = jnp.zeros((head_count, length), F32)
        for h in range(head_count):
            rate = jnp.where(head_index == h, decay_ref[g, h], rate)
        keep = slice(g * head_count, (g + 1) * head_count)
        step_rows[keep, :] = soft
        decay_rows[keep, :] = position_v[g] - jnp.exp(rate) * soft
    line = lax.broadcasted_iota(jnp.int32, (length, length), 0)
    across = lax.broadcasted_iota(jnp.int32, (length, length), 1)
    upto = jnp.where(line <= across, 1.0, 0.0).astype(BF16)
    decays = decay_rows[...]
    high = decays.astype(BF16)
    middle = (decays - high.astype(F32)).astype(BF16)
    low = (decays - high.astype(F32) - middle.astype(F32)).astype(BF16)
    running = dot(high, upto) + (dot(middle, upto) + dot(low, upto))
    rows_kept = running.shape[0]
    total_decay = running[:, length - 1 : length]
    log_step = jnp.log(step_rows[...])
    offset_rows = running - log_step
    tail_rows = jnp.exp(total_decay - offset_rows)
    factors = jnp.exp(total_decay)
    running_columns = jnp.transpose(
        jnp.concatenate([running, jnp.zeros((LANES - rows_kept, length), F32)], axis=0)
    )
    factor_rows = []
    for _, _, heads in columns:
        parts = [jnp.broadcast_to(factors[h : h + 1, :], (1, LANES)) for h in heads]
        factor_rows.append(spread(parts))
    for j, value in enumerate(factor_rows):
        factor_out[j : j + 1, :] = value

    @pl.when(me_s > 0)
    def _():
        for copy in rim_copies():
            copy.wait_recv()

    convolve(0, RIM)

    key_turned = jnp.transpose(key_mix[...])
    for j, (_, _, heads) in enumerate(columns):
        parts = [
            dot((key_turned * tail_rows[h : h + 1, :]).astype(BF16), mix_low[j]) for h in heads
        ]
        states[j] = spread(parts)

    partner = me_s + 1 - 2 * core

    def pair_copy(j):
        if j == column_count:
            return remote(
                factor_out, factor_in, pair_send.at[j], pair_recv.at[j], (partner, me_t)
            )
        return remote(
            state_out.at[j], pair_in.at[j], pair_send.at[j], pair_recv.at[j], (partner, me_t)
        )

    @pl.when(core == 0)
    def _():
        pair_copy(column_count).start()
        for j in range(column_count):
            state_out[j] = states[j].astype(BF16)
            pair_copy(j).start()

    scores[...] = dot(query_mix[...], key_turned.astype(BF16))
    half = length // 2
    below = lax.broadcasted_iota(jnp.int32, (half, half), 0)
    beside = lax.broadcasted_iota(jnp.int32, (half, half), 1)
    causal = below >= beside

    def direct_row(heads):
        parts = []
        for h in heads:
            value = direct_ref[h // head_count, h % head_count]
            parts.append(jnp.full((1, LANES), value, F32))
        return spread(parts)

    def inside(j):
        heads = columns[j][2]
        parts = []
        for h in heads:
            up_to = running_columns[:, h : h + 1]
            since = offset_rows[h : h + 1, :]
            top = jnp.where(causal, up_to[:half] - since[:, :half], -1e30)
            left = up_to[half:] - since[:, :half]
            right = jnp.where(causal, up_to[half:] - since[:, half:], -1e30)
            upper = dot(
                (scores[:half, :half] * jnp.exp(top)).astype(BF16), mix_low[j, :half, :]
            )
            lower = dot(
                (scores[half:, :half] * jnp.exp(left)).astype(BF16), mix_low[j, :half, :]
            ) + dot((scores[half:, half:] * jnp.exp(right)).astype(BF16), mix_low[j, half:, :])
            parts.append((upper, lower))
        direct = direct_row(heads)
        base[j, :half, :] = spread([p[0] for p in parts]) + direct * mix[j, :half, :]
        base[j, half:, :] = spread([p[1] for p in parts]) + direct * mix[j, half:, :]

    early = min(2, column_count)
    for j in range(early):
        inside(j)

    def chain_copy(j):
        return remote(
            chain_out.at[j], chain_in.at[j], chain_send.at[j], chain_recv.at[j], (me_s + 2, me_t)
        )

    def relay_copy(j):
        return remote(
            chain_in.at[j], chain_in.at[j], relay_send.at[j], relay_recv.at[j], (me_s - 1, me_t)
        )

    @pl.when(core == 1)
    def _():
        pair_copy(column_count).wait_recv()
        for j in range(column_count):
            pair_copy(j).wait_recv()
            states[j] += factor_out[j : j + 1, :] * pair_in[j].astype(F32)

    @pl.when(jnp.logical_and(core == 1, plane == 0))
    def _():
        for j in range(column_count):
            if planes > 1:
                chain_out[j] = states[j].astype(BF16)
                chain_copy(j).start()
            enter[j] = pair_in[j]

    @pl.when(jnp.logical_and(core == 0, plane == 0))
    def _():
        enter[...] = jnp.zeros(enter.shape, BF16)

    for j in range(early, column_count):
        inside(j)

    for load in loads[10:16]:
        load.wait()

    for j, (offset, size, _) in enumerate(columns):
        source = wide_gate_v if j < wide_columns else narrow_gate_v
        value = padded(source[:, offset : offset + size]).astype(F32)
        gate_act[j] = value * sigmoid(value)

    @pl.when(jnp.logical_and(core == 1, plane > 0))
    def _():
        for j in range(column_count):
            chain_copy(j).wait_recv()
            relay_copy(j).start()
            carried = chain_in[j].astype(F32)
            moved = factor_in[j : j + 1, :] * carried

            @pl.when(plane < planes - 1)
            def _():
                chain_out[j] = (states[j] + factor_out[j : j + 1, :] * moved).astype(BF16)
                chain_copy(j).start()

            enter[j] = (pair_in[j].astype(F32) + moved).astype(BF16)

    order = lax.broadcasted_iota(jnp.int32, (experts, length), 0)
    order = jnp.where(order == 0, 0, jnp.where(order == experts - 1, 1, order + 1))
    place = plane + lax.shift_right_logical(order, 1)
    place = jnp.where(place >= planes, place - planes, place)
    flip = core + (order & 1)
    flip = jnp.where(flip >= 2, flip - 2, flip)
    named = place * 2 + flip
    member = jnp.zeros((experts, length), F32)
    weight_rows = jnp.zeros((experts, length), F32)
    for k in range(routes_v.shape[0]):
        hit = routes_v[k : k + 1, :] == named
        member = jnp.where(hit, 1.0, member)
        weight_rows = jnp.where(hit, route_weights_v[k : k + 1, :], weight_rows)
    before = jnp.where(line < across, 1.0, 0.0).astype(BF16)
    ranks = dot(member.astype(BF16), before)
    ranks = jnp.where(member > 0.5, ranks, -1.0)
    slots = lax.broadcasted_iota(jnp.int32, (capacity, length), 0).astype(F32)
    slot_lanes = lax.broadcasted_iota(jnp.int32, (length, capacity), 1).astype(F32)
    filler = [jnp.zeros((LANES - experts, length), F32)] if experts < LANES else []
    rank_columns = jnp.transpose(jnp.concatenate([ranks] + filler, axis=0))
    weight_columns = jnp.transpose(jnp.concatenate([weight_rows] + filler, axis=0))
    for d in range(experts):
        chooser[d] = jnp.where(slots == ranks[d : d + 1, :], 1.0, 0.0).astype(BF16)
        weights = jnp.where(
            slot_lanes == rank_columns[:, d : d + 1], weight_columns[:, d : d + 1], 0.0
        )
        rounded = weights.astype(BF16)
        weight_high[d] = rounded
        weight_low[d] = (weights - rounded.astype(F32)).astype(BF16)

    @pl.when(jnp.logical_and(core == 0, plane > 0))
    def _():
        for j in range(column_count):
            relay_copy(j).wait_recv()
            enter[j] = chain_in[j]

    for j, (offset, size, heads) in enumerate(columns):
        wide = j < wide_columns
        grown = spread([jnp.exp(running_columns[:, h : h + 1]) for h in heads])
        value = (base[j] + grown * dot(query_mix[...], enter[j])) * gate_act[j]
        square = value * value
        if len(heads) == 1:
            total = jnp.sum(square, axis=1, keepdims=True)
        else:
            first = jnp.sum(jnp.where(lane < NARROW_HEAD_DIM, square, 0.0), axis=1, keepdims=True)
            rest = jnp.sum(jnp.where(lane < NARROW_HEAD_DIM, 0.0, square), axis=1, keepdims=True)
            total = spread([first, rest])
        value = value * lax.rsqrt(total / (size // len(heads)) + NORM_EPS)
        gains = padded((wide_gain if wide else narrow_gain)[:, offset : offset + size])
        value = (value * gains).astype(BF16)
        start = offset if wide else wide_width + offset
        head_out[:, start : start + size] = value[:, :size]

    for load in loads[16:20]:
        load.wait()

    def first_copy(bundle, dim, k, other, d):
        part, in1, _, _, sems, _ = bundle
        rows = in1.shape[4]
        if dim == 0:
            block = at((col + k) % side, (row + other) % side)
            peer = at((col + k) % side, row)
        else:
            block = at((col + other) % side, (row + k) % side)
            peer = at(col, (row + k) % side)
        return remote(
            part.at[d, block, pl.ds(dim * rows, rows)],
            in1.at[dim, k - 1, other, d],
            sems.at[0, dim, k - 1, other, d],
            sems.at[1, dim, k - 1, other, d],
            (me_s, peer),
        )

    def second_copy(bundle, dim, k, d):
        _, _, mid, in2, _, sems = bundle
        peer = at(col, (row + k) % side) if dim == 0 else at((col + k) % side, row)
        return remote(
            mid.at[dim, k - 1, d],
            in2.at[dim, k - 1, d],
            sems.at[0, dim, k - 1, d],
            sems.at[1, dim, k - 1, d],
            (me_s, peer),
        )

    def scatter(bundle, d, produce):
        part = bundle[0]
        shifts = [(a, b) for a in range(side) for b in range(side)]
        shifts.sort(key=lambda s: -((s[0] > 0) + (s[1] > 0)))
        for a, b in shifts:
            block = at((col + a) % side, (row + b) % side)
            part[d, block] = produce(block).astype(BF16)
            if a:
                first_copy(bundle, 0, a, b, d).start()
            if b:
                first_copy(bundle, 1, b, a, d).start()

    def forward(bundle, d):
        part, in1, mid, _, _, _ = bundle
        rows = in1.shape[4]
        for k in peers:
            for dim in range(2):
                block = at(col, (row + k) % side) if dim == 0 else at((col + k) % side, row)
                total = part[d, block, dim * rows : (dim + 1) * rows].astype(F32)
                for j in peers:
                    first_copy(bundle, dim, j, k, d).wait_recv()
                    total = total + in1[dim, j - 1, k, d].astype(F32)
                mid[dim, k - 1, d] = total.astype(BF16)
                second_copy(bundle, dim, k, d).start()

    def gathered(bundle, dim, d):
        part, in1, _, in2, _, _ = bundle
        rows = in1.shape[4]
        total = part[d, me_t, dim * rows : (dim + 1) * rows].astype(F32)
        for j in peers:
            first_copy(bundle, dim, j, 0, d).wait_recv()
            total = total + in1[dim, j - 1, 0, d].astype(F32)
        for k in peers:
            second_copy(bundle, dim, k, d).wait_recv()
            total = total + in2[dim, k - 1, d].astype(F32)
        return total

    def sent(bundle, d):
        for k in peers:
            for dim in range(2):
                for other in range(side):
                    first_copy(bundle, dim, k, other, d).wait_send()
                second_copy(bundle, dim, k, d).wait_send()

    def project(block):
        lanes = pl.ds(pl.multiple_of(block * width, LANES), width)
        return dot(head_out[...], head_rows_v[:, lanes])

    heads_bundle = (head_part, head_in1, head_mid, head_in2, head_sems, head_sems2)
    sums_bundle = (partial, sum_in1, sum_mid, sum_in2, sum_sems, sum_sems2)
    scatter(heads_bundle, 0, project)
    forward(heads_bundle, 0)
    for dim in range(2):
        keep = slice(dim * half, (dim + 1) * half)
        value = gathered(heads_bundle, dim, 0) + resid_v[keep, :].astype(F32)
        hidden[keep, :] = value
        hidden_low[keep, :] = value.astype(BF16)

    def pick(d):
        return dot(chooser[d], hidden_low[...]).astype(BF16)

    def target(d):
        index = d % (experts - 1) + 1
        return ((plane + index // 2) % planes) * 2 + (core + index % 2) % 2

    def source(d):
        index = d % (experts - 1) + 1
        return ((plane + planes - index // 2) % planes) * 2 + (core + index % 2) % 2

    def slot(d):
        return pl.ds((d % sources) * capacity, capacity)

    def dispatch_copy(d):
        return remote(
            dispatch_out.at[d],
            tokens.at[me_t, d // sources, slot(d)],
            dispatch_send.at[d],
            dispatch_recv.at[d],
            (target(d), me_t),
        )

    def done_copy(d):
        return remote(
            done_out.at[d // sources, slot(d)],
            done_in.at[d],
            done_send.at[d],
            done_recv.at[d],
            (source(d), me_t),
        )

    def send_dispatch(d, c):
        dispatch_out[d] = pick(d)
        dispatch_copy(d).start()
        return c

    tokens[me_t, 0, :capacity] = pick(0)

    def own_copy(dim, k, d):
        part = tokens.at[me_t, d]
        peer = at((col + k) % side, row) if dim == 0 else at(col, (row + k) % side)
        return remote(
            part, part, own_send.at[dim, k - 1, d], own_recv.at[dim, k - 1, d], (me_s, peer)
        )

    rows = tokens.shape[2] // 2

    def pass_copy(dim, j, k, d):
        if dim == 0:
            block = at((col + side - j) % side, row)
            peer = at(col, (row + k) % side)
        else:
            block = at(col, (row + side - j) % side)
            peer = at((col + k) % side, row)
        part = tokens.at[block, d, pl.ds(dim * rows, rows)]
        return remote(
            part,
            part,
            pass_send.at[dim, j - 1, k - 1, d],
            pass_recv.at[dim, j - 1, k - 1, d],
            (me_s, peer),
        )

    def expert(d):
        pieces = [tokens[j, d].astype(F32) for j in range(shards)]
        square = jnp.zeros((2 * rows, 1), F32)
        for piece in pieces:
            square = square + jnp.sum(piece * piece, axis=1, keepdims=True)
        scale = lax.rsqrt(square / (shards * width) + NORM_EPS)
        normed = jnp.concatenate(
            [
                (piece * scale * gain_v[:, j * width : (j + 1) * width]).astype(BF16)
                for j, piece in enumerate(pieces)
            ],
            axis=1,
        )
        gate = dot(normed, gate_v[...])
        up = dot(normed, up_v[...])
        clamped = jnp.minimum(gate, CLAMP_LIMIT)
        act = (
            (jnp.clip(up, -CLAMP_LIMIT, CLAMP_LIMIT) + 1.0)
            * clamped
            * sigmoid(SIGMOID_SCALE * clamped)
        ).astype(BF16)

        def down(block):
            lanes = pl.ds(pl.multiple_of(block * width, LANES), width)
            return dot(act, down_v[:, lanes])

        scatter(sums_bundle, d, down)

    def combine(d, block):
        hidden[...] += dot(weight_high[d], block) + dot(weight_low[d], block)

    def within(value):
        return jnp.logical_and(value >= 0, value < groups)

    def take_done(d, c):
        @pl.when(d == 0)
        def _():
            combine(0, done_out[0, :capacity])

        @pl.when(d > 0)
        def _():
            done_copy(d).wait_recv()
            combine(d, done_in[d])

        return c

    lag = 6

    def step(i, c):
        @pl.when(within(i - 1))
        def _():
            for k in peers:
                for dim in range(2):
                    own_copy(dim, k, i - 1).wait_recv()
            for dim in range(2):
                for j in peers:
                    for k in peers:
                        pass_copy(dim, j, k, i - 1).start()

        @pl.when(i < groups)
        def _():
            def arrive(d, c):
                @pl.when(d > 0)
                def _():
                    dispatch_copy(d).wait_recv()

                return c

            lax.fori_loop(i * sources, (i + 1) * sources, arrive, 0)
            for k in peers:
                for dim in range(2):
                    own_copy(dim, k, i).start()

        @pl.when(i == 0)
        def _():
            if sources == 1:
                lax.fori_loop(1, experts, send_dispatch, 0)
            for load in loads[20:]:
                load.wait()

        @pl.when(within(i - 3))
        def _():
            forward(sums_bundle, i - 3)

        @pl.when(within(i - 2))
        def _():
            for dim in range(2):
                for j in peers:
                    for k in peers:
                        pass_copy(dim, j, k, i - 2).wait_recv()
            expert(i - 2)

        @pl.when(within(i - 4))
        def _():
            for dim in range(2):
                done_out[i - 4, dim * rows : (dim + 1) * rows] = gathered(
                    sums_bundle, dim, i - 4
                ).astype(BF16)

            def leave(d, c):
                @pl.when(d > 0)
                def _():
                    done_copy(d).start()

                return c

            lax.fori_loop((i - 4) * sources, (i - 3) * sources, leave, 0)

        @pl.when(within(i - lag))
        def _():
            lax.fori_loop((i - lag) * sources, (i - lag + 1) * sources, take_done, 0)

        return c

    steps = groups + 4
    if sources > 1:
        lax.fori_loop(1, experts, send_dispatch, 0)
    lax.fori_loop(0, steps, step, 0)
    lax.fori_loop((steps - lag) * sources, experts, take_done, 0)
    out_ref[...] = hidden[...].astype(BF16)

    @pl.when(me_s < experts - 1)
    def _():
        for copy in rim_copies():
            copy.wait_send()

    @pl.when(core == 0)
    def _():
        for j in range(column_count + 1):
            pair_copy(j).wait_send()

    @pl.when(jnp.logical_and(core == 1, plane < planes - 1))
    def _():
        for j in range(column_count):
            chain_copy(j).wait_send()

    @pl.when(jnp.logical_and(core == 1, plane > 0))
    def _():
        for j in range(column_count):
            relay_copy(j).wait_send()

    sent(heads_bundle, 0)

    def finish_sp(d, c):
        dispatch_copy(d).wait_send()
        done_copy(d).wait_send()
        return c

    lax.fori_loop(1, experts, finish_sp, 0)

    def finish_group(d, c):
        for dim in range(2):
            for j in peers:
                own_copy(dim, j, d).wait_send()
                for k in peers:
                    pass_copy(dim, j, k, d).wait_send()
        sent(sums_bundle, d)
        return c

    lax.fori_loop(0, groups, finish_group, 0)


def layer_call(side, experts, arrays):
    resid, narrow, wide, key = arrays[:4]
    step, decay = arrays[7], arrays[8]
    gate, up, down = arrays[22:]
    routes = arrays[20]
    length = resid.shape[0]
    shards = side * side
    width = resid.shape[1] // shards
    capacity = 4 * length * routes.shape[0] // (3 * experts)
    sources = max(1, min(experts, 128 // capacity))
    groups = experts // sources
    rows = sources * capacity
    state = key.shape[1] // GROUPS
    wide_width, narrow_width = wide.shape[1], narrow.shape[1]
    column_count = wide_width // LANES + -(-narrow_width // LANES)
    head_rows = wide_width + narrow_width
    near = side - 1
    tap_count = arrays[11].shape[0]
    vmem = pltpu.VMEM
    dma = pltpu.SemaphoreType.DMA
    scratch = [
        vmem((RIM + length, wide_width + 2 * state), BF16),
        vmem((RIM + length, narrow_width), BF16),
        vmem((length, wide_width), BF16),
        vmem((length, narrow_width), BF16),
        vmem(step.shape, BF16),
        vmem(step.shape, F32),
        vmem((tap_count, narrow_width), F32),
        vmem((tap_count, wide_width), F32),
        vmem((tap_count, state), F32),
        vmem((tap_count, state), F32),
        vmem((1, narrow_width), F32),
        vmem((1, wide_width), F32),
        vmem((head_rows, resid.shape[1]), BF16),
        vmem((1, resid.shape[1]), F32),
        vmem(routes.shape, jnp.int32),
        vmem(routes.shape, F32),
        vmem((length, width), BF16),
        vmem(gate.shape[1:], BF16),
        vmem(up.shape[1:], BF16),
        vmem(down.shape[1:], BF16),
        vmem((8, length), F32),
        vmem((8, length), F32),
        vmem((column_count, length, LANES), F32),
        vmem((column_count, length, LANES), BF16),
        vmem((length, state), F32),
        vmem((length, state), BF16),
        vmem((length, length), F32),
        vmem((column_count, length, LANES), F32),
        vmem((column_count, length, LANES), F32),
        vmem((column_count, state, LANES), F32),
        vmem((column_count, state, LANES), BF16),
        vmem((column_count, state, LANES), BF16),
        vmem((column_count, state, LANES), BF16),
        vmem((column_count, state, LANES), BF16),
        vmem((column_count, state, LANES), BF16),
        vmem((8, LANES), F32),
        vmem((8, LANES), F32),
        vmem((length, head_rows), BF16),
        vmem((1, shards, length, width), BF16),
        vmem((2, near, side, 1, length // 2, width), BF16),
        vmem((2, near, 1, length // 2, width), BF16),
        vmem((2, near, 1, length // 2, width), BF16),
        vmem((length, width), F32),
        vmem((length, width), BF16),
        vmem((experts, capacity, length), BF16),
        vmem((experts, length, capacity), BF16),
        vmem((experts, length, capacity), BF16),
        vmem((experts, capacity, width), BF16),
        vmem((shards, groups, rows, width), BF16),
        vmem((groups, shards, rows, width), BF16),
        vmem((2, near, side, groups, rows // 2, width), BF16),
        vmem((2, near, groups, rows // 2, width), BF16),
        vmem((2, near, groups, rows // 2, width), BF16),
        vmem((groups, rows, width), BF16),
        vmem((experts, capacity, width), BF16),
        dma((23,)),
        dma((2,)),
        dma((2,)),
        dma((column_count + 1,)),
        dma((column_count + 1,)),
        dma((column_count,)),
        dma((column_count,)),
        dma((column_count,)),
        dma((column_count,)),
        dma((2, 2, near, side, 1)),
        dma((2, 2, near, 1)),
        dma((experts,)),
        dma((experts,)),
        dma((2, near, groups)),
        dma((2, near, groups)),
        dma((2, near, near, groups)),
        dma((2, near, near, groups)),
        dma((2, 2, near, side, groups)),
        dma((2, 2, near, groups)),
        dma((experts,)),
        dma((experts,)),
    ]
    hbm = pl.BlockSpec(memory_space=pl.ANY)
    smem = pl.BlockSpec(memory_space=pltpu.SMEM)
    specs = [hbm] * len(arrays)
    specs[8] = smem
    specs[10] = smem
    return pl.pallas_call(
        functools.partial(layer_kernel, side, experts, capacity),
        out_shape=jax.ShapeDtypeStruct((length, width), BF16),
        in_specs=specs,
        out_specs=pl.BlockSpec(memory_space=pltpu.VMEM),
        scratch_shapes=scratch,
        compiler_params=pltpu.CompilerParams(
            collective_id=0, has_side_effects=True, vmem_limit_bytes=60 * 1024 * 1024
        ),
    )(*arrays)


def local(*arrays):
    arrays = list(arrays)
    shards = lax.axis_size("tp")
    side = int(round(shards**0.5))
    assert side * side == shards
    for i in (7, 9):
        arrays[i] = jnp.transpose(arrays[i], (1, 2, 0))
    for i in (15, 16, 19):
        arrays[i] = arrays[i][None, :]
    for i in (20, 21):
        arrays[i] = jnp.transpose(arrays[i])
    return layer_call(side, lax.axis_size("sp"), arrays)


def solution(mesh):
    return jax.shard_map(
        local,
        mesh=mesh,
        in_specs=(
            P("sp", None),
            P("sp", "tp"),
            P("sp", "tp"),
            P("sp", None),
            P("sp", None),
            P("sp", "tp"),
            P("sp", "tp"),
            P("sp", None, "tp"),
            P(None, "tp"),
            P("sp", None, "tp"),
            P(None, "tp"),
            P(None, "tp"),
            P(None, "tp"),
            P(),
            P(),
            P("tp"),
            P("tp"),
            P("tp", None),
            P("tp", None),
            P(),
            P("sp", None),
            P("sp", None),
            P("sp", None, "tp"),
            P("sp", None, "tp"),
            P("sp", "tp", None),
        ),
        out_specs=P("sp", "tp"),
        check_vma=False,
    )
```

time: 215 us -> 115 us (0.53)
  other arithmetic: 23.1 us -> 0 us
  local copies, waits for them, and re-layouts: 21.9 us -> 1.67 us
  blocking collectives: 18.4 us -> 0 us
  between operations: 14.1 us -> 0.01 us
  waiting for transfers between devices: 13.5 us -> 0 us
  matrix products: 9.09 us -> 0 us
  starting transfers between devices: 2.41 us -> 0 us
    all_gather x1 -> x0, blocking collectives: 18.4 us -> none  [entering(): lax.all_gather((narrow_packed, wide_states.astype(jnp.bfloat16)), axis)]
    all_gather x1 -> x0, waiting for transfers between devices: 13.5 us -> none  [entering(): lax.all_gather((narrow_packed, wide_states.astype(jnp.bfloat16)), axis)]
    dot_general x8 -> x0, matrix products: 9.09 us -> none  [the longest x2 4.05 us: finish_head(): jnp.einsum('bln,bnp->blp', query_blocks * jnp.exp(cum_decay)[..., None],...]
    slice x15 -> x0, local copies, waits for them, and re-layouts: 6.7 us -> none  [the longest x4 3.01 us: local(): stream[length - rim_len:]]
    dynamic_slice x8 -> x0, local copies, waits for them, and re-layouts: 4.59 us -> none  [the longest x2 2.22 us: own_group(): return lax.dynamic_slice_in_dim(table, group_column, state_size, 1)]
    reduce_sum x7 -> x0, other arithmetic: 4.52 us -> none  [the longest x2 2.39 us: carry(): jnp.sum(factor[:, :, None, None] * states.astype(jnp.float32), axis=0)]
    mul x9 -> x0, other arithmetic: 4.17 us -> none  [the longest x4 1.62 us: conv_with_rim(): return jax.nn.silu(accumulated)]
    convert_element_type x9 -> x0, other arithmetic: 3.21 us -> none  [the longest x2 1.42 us: group_out(): (result.reshape(length, head_count * head_dimension) * norm_gain_vector)....]
  transfers between devices with their start and end apart: 2 -> 0, of which waited for: 1 -> 0; matrix products, arithmetic and copies ran while one was open for 14% -> 0% of each run, Pallas kernels for 0% -> 0%
where the time goes in v1:
time: 115 us; the launch traced here: 113 us
  Pallas kernels  111 us (97%)
  local copies, waits for them, and re-layouts  1.67 us (1%)
    pallas_call x1, Pallas kernels, layer_call(): pl.pallas_call(functools.partial(layer_kernel, side, experts, capacity),...  111 us

profile of v1, /device:TPU:0, one launch (start us, length us, event | category | flops | bytes accessed | tf_op | source)
XLA Modules:
  0.0 112.7 jit_solution(849683998813075580)
XLA Ops:
  0.0 111.0 %shard_map.235 = bf16[256,512]{1,0:T(8,128)(2,1)} custom-call(bf16[256,2048]{1,0:T(8,128)(2,1)} %resid_hbm.1, bf16[256,256]{1,0:T(8,128)(2,1)} %narrow_hbm.1, bf16[256,512]{1,0:T(8,128)(2,1)} %wide_hbm.1, bf16[256,512]{1,0:T(8,128)(2,1)} %key_hbm.1, bf16[256,512]{1,0:T(8,128)(2,1)} %query_hbm.1, bf16[256,256]{1,0:T(8,128)(2,1)} %narrow_gate_hbm.1, ...), custom_call_target="tpu_custom_call" | custom-call | tf_op jit(solution)/shard_map/pallas_call | solution.py:930
  111.0 1.7 %copy.27 = bf16[256,512]{1,0:T(8,128)(2,1)} copy(bf16[256,512]{1,0:T(8,128)(2,1)} %shard_map.235) | data formatting | bytes 524288

commit v2 on v1

--- a/solution.py
+++ b/solution.py
@@ -12,6 +12,7 @@
 GROUPS = 4
 LANES = 128
 RIM = 16
+FAR_GROUPS = 2
 
 NORM_EPS = 1e-06
 CLAMP_LIMIT = 7.0
@@ -58,6 +59,8 @@
     up_hbm,
     down_hbm,
     out_ref,
+    rim_wide,
+    rim_narrow,
     wide_in,
     narrow_in,
     wide_gate_v,
@@ -101,7 +104,6 @@
     head_mid,
     head_in2,
     hidden,
-    hidden_low,
     chooser,
     weight_high,
     weight_low,
@@ -113,6 +115,10 @@
     sum_in2,
     done_out,
     done_in,
+    full,
+    partner_out,
+    far_out,
+    out_v,
     load_sem,
     rim_send,
     rim_recv,
@@ -123,15 +129,13 @@
     relay_send,
     relay_recv,
     head_sems,
-    head_sems2,
+    early_sems,
     dispatch_send,
     dispatch_recv,
-    own_send,
-    own_recv,
-    pass_send,
-    pass_recv,
+    far_send,
+    far_recv,
+    token_sems,
     sum_sems,
-    sum_sems2,
     done_send,
     done_recv,
 ):
@@ -180,34 +184,53 @@
     own_columns = pl.ds(pl.multiple_of(me_t * width, LANES), width)
     group_slice = pl.ds(group_column, state)
     body = pl.ds(RIM, length)
+    edge = pl.ds(length - RIM, RIM)
+    wide_part = pl.ds(0, wide_width)
+    key_part = pl.ds(wide_width, state)
+    query_part = pl.ds(wide_width + state, state)
     moves = (
-        (wide_hbm, wide_in.at[body, pl.ds(0, wide_width)]),
-        (key_hbm.at[:, group_slice], wide_in.at[body, pl.ds(wide_width, state)]),
-        (query_hbm.at[:, group_slice], wide_in.at[body, pl.ds(wide_width + state, state)]),
-        (narrow_hbm, narrow_in.at[body]),
-        (wide_taps_hbm, wide_taps),
-        (key_taps_hbm.at[:, group_slice], key_taps),
-        (query_taps_hbm.at[:, group_slice], query_taps),
-        (narrow_taps_hbm, narrow_taps),
-        (step_hbm, step_v),
-        (position_hbm, position_v),
-        (wide_gate_hbm, wide_gate_v),
-        (narrow_gate_hbm, narrow_gate_v),
-        (narrow_gain_hbm, narrow_gain),
-        (wide_gain_hbm, wide_gain),
-        (routes_hbm, routes_v),
-        (route_weights_hbm, route_weights_v),
-        (wide_rows_hbm, head_rows_v.at[pl.ds(0, wide_width)]),
-        (narrow_rows_hbm, head_rows_v.at[pl.ds(wide_width, narrow_width)]),
-        (resid_hbm.at[:, own_columns], resid_v),
-        (gain_hbm, gain_v),
-        (gate_hbm.at[0], gate_v),
-        (up_hbm.at[0], up_v),
-        (down_hbm.at[0], down_v),
+        (0, wide_hbm.at[edge], rim_wide.at[:, wide_part]),
+        (0, key_hbm.at[edge, group_slice], rim_wide.at[:, key_part]),
+        (0, query_hbm.at[edge, group_slice], rim_wide.at[:, query_part]),
+        (1, narrow_hbm.at[edge], rim_narrow),
+        (2, wide_hbm, wide_in.at[body, wide_part]),
+        (2, key_hbm.at[:, group_slice], wide_in.at[body, key_part]),
+        (2, query_hbm.at[:, group_slice], wide_in.at[body, query_part]),
+        (3, narrow_hbm, narrow_in.at[body]),
+        (4, wide_taps_hbm, wide_taps),
+        (5, key_taps_hbm.at[:, group_slice], key_taps),
+        (6, query_taps_hbm.at[:, group_slice], query_taps),
+        (7, narrow_taps_hbm, narrow_taps),
+        (8, step_hbm, step_v),
+        (9, position_hbm, position_v),
+        (10, wide_gate_hbm, wide_gate_v),
+        (11, narrow_gate_hbm, narrow_gate_v),
+        (12, narrow_gain_hbm, narrow_gain),
+        (13, wide_gain_hbm, wide_gain),
+        (14, routes_hbm, routes_v),
+        (15, route_weights_hbm, route_weights_v),
+        (16, wide_rows_hbm, head_rows_v.at[wide_part]),
+        (16, narrow_rows_hbm, head_rows_v.at[pl.ds(wide_width, narrow_width)]),
+        (17, resid_hbm.at[:, own_columns], resid_v),
+        (18, gain_hbm, gain_v),
+        (19, gate_hbm.at[0], gate_v),
+        (20, up_hbm.at[0], up_v),
+        (21, down_hbm.at[0], down_v),
     )
-    loads = [pltpu.make_async_copy(s, d, load_sem.at[i]) for i, (s, d) in enumerate(moves)]
-    for load in loads:
-        load.start()
+    whole = {0: rim_wide, 2: wide_in.at[body], 16: head_rows_v}
+
+    def load(first, last):
+        for i, source, target in moves:
+            if first <= i < last:
+                pltpu.make_async_copy(source, target, load_sem.at[i]).start()
+
+    def spent(ref, sem):
+        pltpu.make_async_copy(ref, ref, sem).wait()
+
+    def loaded(first, last):
+        for i in range(first, last):
+            ref = whole.get(i, [m[2] for m in moves if m[0] == i][0])
+            spent(ref, load_sem.at[i])
 
     barrier = pltpu.get_barrier_semaphore()
 
@@ -220,23 +243,22 @@
         greet((me_s + d) % experts, me_t)
         return c
 
+    load(0, 2)
     lax.fori_loop(1, experts, greet_sp, 0)
     for k in peers:
         greet(me_s, at((col + k) % side, row))
         greet(me_s, at(col, (row + k) % side))
+    load(2, 16)
+    loaded(0, 2)
     pl.semaphore_wait(barrier, experts - 1 + 2 * (side - 1))
 
-    for load in loads[:4]:
-        load.wait()
-
-    tail = pl.ds(length, RIM)
     head = pl.ds(0, RIM)
 
     def rim_copies():
         where = (me_s + 1, me_t)
         return (
-            remote(wide_in.at[tail], wide_in.at[head], rim_send.at[0], rim_recv.at[0], where),
-            remote(narrow_in.at[tail], narrow_in.at[head], rim_send.at[1], rim_recv.at[1], where),
+            remote(rim_wide, wide_in.at[head], rim_send.at[0], rim_recv.at[0], where),
+            remote(rim_narrow, narrow_in.at[head], rim_send.at[1], rim_recv.at[1], where),
         )
 
     @pl.when(me_s < experts - 1)
@@ -249,8 +271,8 @@
         wide_in[:RIM, :] = jnp.zeros((RIM, wide_in.shape[1]), BF16)
         narrow_in[:RIM, :] = jnp.zeros((RIM, narrow_in.shape[1]), BF16)
 
-    for load in loads[4:10]:
-        load.wait()
+    load(16, 22)
+    loaded(2, 10)
 
     def padded(v):
         if v.shape[1] == LANES:
@@ -332,6 +354,40 @@
     for j, value in enumerate(factor_rows):
         factor_out[j : j + 1, :] = value
 
+    loaded(10, 16)
+
+    for j, (offset, size, _) in enumerate(columns):
+        source = wide_gate_v if j < wide_columns else narrow_gate_v
+        value = padded(source[:, offset : offset + size]).astype(F32)
+        gate_act[j] = value * sigmoid(value)
+
+    order = lax.broadcasted_iota(jnp.int32, (experts, length), 0)
+    mask = jnp.where(order < experts - 3, order + 3, order + 5 - experts)
+    mask = jnp.where(order == 0, 1, jnp.where(order == experts - 1, 0, mask))
+    named = mask ^ me_s
+    member = jnp.zeros((experts, length), F32)
+    weight_rows = jnp.zeros((experts, length), F32)
+    for k in range(routes_v.shape[0]):
+        hit = routes_v[k : k + 1, :] == named
+        member = jnp.where(hit, 1.0, member)
+        weight_rows = jnp.where(hit, route_weights_v[k : k + 1, :], weight_rows)
+    before = jnp.where(line < across, 1.0, 0.0).astype(BF16)
+    ranks = dot(member.astype(BF16), before)
+    ranks = jnp.where(member > 0.5, ranks, -1.0)
+    slots = lax.broadcasted_iota(jnp.int32, (capacity, length), 0).astype(F32)
+    slot_lanes = lax.broadcasted_iota(jnp.int32, (length, capacity), 1).astype(F32)
+    filler = [jnp.zeros((LANES - experts, length), F32)] if experts < LANES else []
+    rank_columns = jnp.transpose(jnp.concatenate([ranks] + filler, axis=0))
+    weight_columns = jnp.transpose(jnp.concatenate([weight_rows] + filler, axis=0))
+    for d in range(experts):
+        chooser[d] = jnp.where(slots == ranks[d : d + 1, :], 1.0, 0.0).astype(BF16)
+        weights = jnp.where(
+            slot_lanes == rank_columns[:, d : d + 1], weight_columns[:, d : d + 1], 0.0
+        )
+        rounded = weights.astype(BF16)
+        weight_high[d] = rounded
+        weight_low[d] = (weights - rounded.astype(F32)).astype(BF16)
+
     @pl.when(me_s > 0)
     def _():
         for copy in rim_copies():
@@ -351,10 +407,10 @@
     def pair_copy(j):
         if j == column_count:
             return remote(
-                factor_out, factor_in, pair_send.at[j], pair_recv.at[j], (partner, me_t)
+                factor_out, factor_in, pair_send.at[1], pair_recv.at[1], (partner, me_t)
             )
         return remote(
-            state_out.at[j], pair_in.at[j], pair_send.at[j], pair_recv.at[j], (partner, me_t)
+            state_out.at[j], pair_in.at[j], pair_send.at[0], pair_recv.at[0], (partner, me_t)
         )
 
     @pl.when(core == 0)
@@ -403,19 +459,19 @@
 
     def chain_copy(j):
         return remote(
-            chain_out.at[j], chain_in.at[j], chain_send.at[j], chain_recv.at[j], (me_s + 2, me_t)
+            chain_out.at[j], chain_in.at[j], chain_send.at[0], chain_recv.at[j], (me_s + 2, me_t)
         )
 
     def relay_copy(j):
         return remote(
-            chain_in.at[j], chain_in.at[j], relay_send.at[j], relay_recv.at[j], (me_s - 1, me_t)
+            chain_in.at[j], chain_in.at[j], relay_send.at[0], relay_recv.at[j], (me_s - 1, me_t)
         )
 
     @pl.when(core == 1)
     def _():
         pair_copy(column_count).wait_recv()
+        spent(pair_in, pair_recv.at[0])
         for j in range(column_count):
-            pair_copy(j).wait_recv()
             states[j] += factor_out[j : j + 1, :] * pair_in[j].astype(F32)
 
     @pl.when(jnp.logical_and(core == 1, plane == 0))
@@ -433,66 +489,21 @@
     for j in range(early, column_count):
         inside(j)
 
-    for load in loads[10:16]:
-        load.wait()
-
-    for j, (offset, size, _) in enumerate(columns):
-        source = wide_gate_v if j < wide_columns else narrow_gate_v
-        value = padded(source[:, offset : offset + size]).astype(F32)
-        gate_act[j] = value * sigmoid(value)
-
-    @pl.when(jnp.logical_and(core == 1, plane > 0))
-    def _():
-        for j in range(column_count):
-            chain_copy(j).wait_recv()
-            relay_copy(j).start()
-            carried = chain_in[j].astype(F32)
-            moved = factor_in[j : j + 1, :] * carried
-
-            @pl.when(plane < planes - 1)
-            def _():
-                chain_out[j] = (states[j] + factor_out[j : j + 1, :] * moved).astype(BF16)
-                chain_copy(j).start()
-
-            enter[j] = (pair_in[j].astype(F32) + moved).astype(BF16)
-
-    order = lax.broadcasted_iota(jnp.int32, (experts, length), 0)
-    order = jnp.where(order == 0, 0, jnp.where(order == experts - 1, 1, order + 1))
-    place = plane + lax.shift_right_logical(order, 1)
-    place = jnp.where(place >= planes, place - planes, place)
-    flip = core + (order & 1)
-    flip = jnp.where(flip >= 2, flip - 2, flip)
-    named = place * 2 + flip
-    member = jnp.zeros((experts, length), F32)
-    weight_rows = jnp.zeros((experts, length), F32)
-    for k in range(routes_v.shape[0]):
-        hit = routes_v[k : k + 1, :] == named
-        member = jnp.where(hit, 1.0, member)
-        weight_rows = jnp.where(hit, route_weights_v[k : k + 1, :], weight_rows)
-    before = jnp.where(line < across, 1.0, 0.0).astype(BF16)
-    ranks = dot(member.astype(BF16), before)
-    ranks = jnp.where(member > 0.5, ranks, -1.0)
-    slots = lax.broadcasted_iota(jnp.int32, (capacity, length), 0).astype(F32)
-    slot_lanes = lax.broadcasted_iota(jnp.int32, (length, capacity), 1).astype(F32)
-    filler = [jnp.zeros((LANES - experts, length), F32)] if experts < LANES else []
-    rank_columns = jnp.transpose(jnp.concatenate([ranks] + filler, axis=0))
-    weight_columns = jnp.transpose(jnp.concatenate([weight_rows] + filler, axis=0))
-    for d in range(experts):
-        chooser[d] = jnp.where(slots == ranks[d : d + 1, :], 1.0, 0.0).astype(BF16)
-        weights = jnp.where(
-            slot_lanes == rank_columns[:, d : d + 1], weight_columns[:, d : d + 1], 0.0
-        )
-        rounded = weights.astype(BF16)
-        weight_high[d] = rounded
-        weight_low[d] = (weights - rounded.astype(F32)).astype(BF16)
-
-    @pl.when(jnp.logical_and(core == 0, plane > 0))
-    def _():
-        for j in range(column_count):
-            relay_copy(j).wait_recv()
-            enter[j] = chain_in[j]
-
-    for j, (offset, size, heads) in enumerate(columns):
+    def carry_odd(j):
+        chain_copy(j).wait_recv()
+        relay_copy(j).start()
+        carried = chain_in[j].astype(F32)
+        moved = factor_in[j : j + 1, :] * carried
+
+        @pl.when(plane < planes - 1)
+        def _():
+            chain_out[j] = (states[j] + factor_out[j : j + 1, :] * moved).astype(BF16)
+            chain_copy(j).start()
+
+        enter[j] = (pair_in[j].astype(F32) + moved).astype(BF16)
+
+    def finish(j):
+        offset, size, heads = columns[j]
         wide = j < wide_columns
         grown = spread([jnp.exp(running_columns[:, h : h + 1]) for h in heads])
         value = (base[j] + grown * dot(query_mix[...], enter[j])) * gate_act[j]
@@ -509,11 +520,25 @@
         start = offset if wide else wide_width + offset
         head_out[:, start : start + size] = value[:, :size]
 
-    for load in loads[16:20]:
-        load.wait()
+    for j in range(column_count):
+
+        @pl.when(jnp.logical_and(core == 1, plane > 0))
+        def _():
+            carry_odd(j)
+
+        @pl.when(jnp.logical_and(core == 0, plane > 0))
+        def _():
+            relay_copy(j).wait_recv()
+            enter[j] = chain_in[j]
+
+        finish(j)
+
+    loaded(16, 19)
+
+    near = side - 1
 
     def first_copy(bundle, dim, k, other, d):
-        part, in1, _, _, sems, _ = bundle
+        part, in1, _, _, sems = bundle
         rows = in1.shape[4]
         if dim == 0:
             block = at((col + k) % side, (row + other) % side)
@@ -524,20 +549,16 @@
         return remote(
             part.at[d, block, pl.ds(dim * rows, rows)],
             in1.at[dim, k - 1, other, d],
-            sems.at[0, dim, k - 1, other, d],
-            sems.at[1, dim, k - 1, other, d],
+            sems.at[0, d],
+            sems.at[1 if other else 2, d],
             (me_s, peer),
         )
 
     def second_copy(bundle, dim, k, d):
-        _, _, mid, in2, _, sems = bundle
+        _, _, mid, in2, sems = bundle
         peer = at(col, (row + k) % side) if dim == 0 else at((col + k) % side, row)
         return remote(
-            mid.at[dim, k - 1, d],
-            in2.at[dim, k - 1, d],
-            sems.at[0, dim, k - 1, d],
-            sems.at[1, dim, k - 1, d],
-            (me_s, peer),
+            mid.at[dim, k - 1, d], in2.at[dim, k - 1, d], sems.at[3, d], sems.at[2, d], (me_s, peer)
         )
 
     def scatter(bundle, d, produce):
@@ -553,114 +574,156 @@
                 first_copy(bundle, 1, b, a, d).start()
 
     def forward(bundle, d):
-        part, in1, mid, _, _, _ = bundle
+        part, in1, mid, _, sems = bundle
         rows = in1.shape[4]
+        spent(part.at[d, pl.ds(0, near * near)], sems.at[1, d])
         for k in peers:
             for dim in range(2):
                 block = at(col, (row + k) % side) if dim == 0 else at((col + k) % side, row)
                 total = part[d, block, dim * rows : (dim + 1) * rows].astype(F32)
                 for j in peers:
-                    first_copy(bundle, dim, j, k, d).wait_recv()
                     total = total + in1[dim, j - 1, k, d].astype(F32)
                 mid[dim, k - 1, d] = total.astype(BF16)
                 second_copy(bundle, dim, k, d).start()
 
+    def settle(bundle, d):
+        spent(bundle[0].at[d, pl.ds(0, 2 * near)], bundle[4].at[2, d])
+
     def gathered(bundle, dim, d):
-        part, in1, _, in2, _, _ = bundle
+        part, in1, _, in2, _ = bundle
         rows = in1.shape[4]
         total = part[d, me_t, dim * rows : (dim + 1) * rows].astype(F32)
         for j in peers:
-            first_copy(bundle, dim, j, 0, d).wait_recv()
             total = total + in1[dim, j - 1, 0, d].astype(F32)
         for k in peers:
-            second_copy(bundle, dim, k, d).wait_recv()
             total = total + in2[dim, k - 1, d].astype(F32)
         return total
 
     def sent(bundle, d):
-        for k in peers:
-            for dim in range(2):
-                for other in range(side):
-                    first_copy(bundle, dim, k, other, d).wait_send()
-                second_copy(bundle, dim, k, d).wait_send()
+        part, sems = bundle[0], bundle[4]
+        spent(part.at[d, pl.ds(0, near * side)], sems.at[0, d])
+        spent(part.at[d, pl.ds(0, near)], sems.at[3, d])
 
     def project(block):
         lanes = pl.ds(pl.multiple_of(block * width, LANES), width)
         return dot(head_out[...], head_rows_v[:, lanes])
 
-    heads_bundle = (head_part, head_in1, head_mid, head_in2, head_sems, head_sems2)
-    sums_bundle = (partial, sum_in1, sum_mid, sum_in2, sum_sems, sum_sems2)
-    scatter(heads_bundle, 0, project)
-    forward(heads_bundle, 0)
-    for dim in range(2):
-        keep = slice(dim * half, (dim + 1) * half)
-        value = gathered(heads_bundle, dim, 0) + resid_v[keep, :].astype(F32)
-        hidden[keep, :] = value
-        hidden_low[keep, :] = value.astype(BF16)
-
-    def pick(d):
-        return dot(chooser[d], hidden_low[...]).astype(BF16)
-
-    def target(d):
-        index = d % (experts - 1) + 1
-        return ((plane + index // 2) % planes) * 2 + (core + index % 2) % 2
-
-    def source(d):
-        index = d % (experts - 1) + 1
-        return ((plane + planes - index // 2) % planes) * 2 + (core + index % 2) % 2
-
-    def slot(d):
-        return pl.ds((d % sources) * capacity, capacity)
-
-    def dispatch_copy(d):
-        return remote(
-            dispatch_out.at[d],
-            tokens.at[me_t, d // sources, slot(d)],
-            dispatch_send.at[d],
-            dispatch_recv.at[d],
-            (target(d), me_t),
-        )
-
-    def done_copy(d):
-        return remote(
-            done_out.at[d // sources, slot(d)],
-            done_in.at[d],
-            done_send.at[d],
-            done_recv.at[d],
-            (source(d), me_t),
-        )
-
-    def send_dispatch(d, c):
-        dispatch_out[d] = pick(d)
-        dispatch_copy(d).start()
-        return c
-
-    tokens[me_t, 0, :capacity] = pick(0)
-
-    def own_copy(dim, k, d):
-        part = tokens.at[me_t, d]
+    def spread_copy(buffer, sems, index, dim, k, d):
+        part = buffer.at[me_t, d]
         peer = at((col + k) % side, row) if dim == 0 else at(col, (row + k) % side)
-        return remote(
-            part, part, own_send.at[dim, k - 1, d], own_recv.at[dim, k - 1, d], (me_s, peer)
-        )
-
-    rows = tokens.shape[2] // 2
-
-    def pass_copy(dim, j, k, d):
+        return remote(part, part, sems.at[0, index], sems.at[1, index], (me_s, peer))
+
+    def pass_copy(buffer, sems, index, dim, j, k, d):
+        rows = buffer.shape[2] // 2
         if dim == 0:
             block = at((col + side - j) % side, row)
             peer = at(col, (row + k) % side)
         else:
             block = at(col, (row + side - j) % side)
             peer = at((col + k) % side, row)
-        part = tokens.at[block, d, pl.ds(dim * rows, rows)]
+        part = buffer.at[block, d, pl.ds(dim * rows, rows)]
+        return remote(part, part, sems.at[2, index], sems.at[3, index], (me_s, peer))
+
+    def spread_start(buffer, sems, d):
+        for k in peers:
+            for dim in range(2):
+                spread_copy(buffer, sems, d, dim, k, d).start()
+
+    def pass_start(buffer, sems, d):
+        for dim in range(2):
+            for j in peers:
+                for k in peers:
+                    pass_copy(buffer, sems, d, dim, j, k, d).start()
+
+    def span(buffer, count, d):
+        return buffer.at[pl.ds(0, count), d]
+
+    heads_bundle = (head_part, head_in1, head_mid, head_in2, head_sems)
+    sums_bundle = (partial, sum_in1, sum_mid, sum_in2, sum_sems)
+    scatter(heads_bundle, 0, project)
+    forward(heads_bundle, 0)
+    settle(heads_bundle, 0)
+    for dim in range(2):
+        keep = slice(dim * half, (dim + 1) * half)
+        value = gathered(heads_bundle, dim, 0) + resid_v[keep, :].astype(F32)
+        hidden[keep, :] = value
+        full[me_t, 0, keep, :] = value.astype(BF16)
+
+    direct = sources == 1
+    own = experts - 1
+    ahead = 2
+    far = own - min(FAR_GROUPS, own - 1)
+    lag = 6
+    own_slots = slice(own % sources * capacity, (own % sources + 1) * capacity)
+
+    def pick(block, d):
+        return dot(chooser[d], full[block, 0]).astype(BF16)
+
+    def mate(d):
+        mask = d + 1 + 2 * ((d + experts - 1) // experts)
+        mask = mask - (experts - 2) * ((d + 3) // experts) - 4 * ((d + 1) // experts)
+        where = me_s
+        bit = 1
+        while bit < experts:
+            where = where + (mask // bit) % 2 * bit * (1 - 2 * ((me_s // bit) % 2))
+            bit *= 2
+        return where
+
+    def slot(d):
+        return pl.ds((d % sources) * capacity, capacity)
+
+    def dispatch_copy(d):
         return remote(
-            part,
-            part,
-            pass_send.at[dim, j - 1, k - 1, d],
-            pass_recv.at[dim, j - 1, k - 1, d],
-            (me_s, peer),
-        )
+            dispatch_out.at[d],
+            tokens.at[me_t, d // sources, slot(d)],
+            dispatch_send.at[0],
+            dispatch_recv.at[d],
+            (mate(d), me_t),
+        )
+
+    def partner_copy():
+        return remote(
+            partner_out,
+            tokens.at[:, 0, pl.ds(0, capacity)],
+            dispatch_send.at[1],
+            dispatch_recv.at[0],
+            (mate(0), me_t),
+        )
+
+    far_blocks = [at((col + j) % side, (row + k) % side) for j in peers for k in peers]
+
+    def far_copy(n, d):
+        return remote(
+            far_out.at[n, d], tokens.at[far_blocks[n], d], far_send.at[0], far_recv.at[d], (mate(d), me_t)
+        )
+
+    def done_copy(d):
+        return remote(
+            done_out.at[d // sources, slot(d)],
+            done_in.at[d],
+            done_send.at[0],
+            done_recv.at[d],
+            (mate(d), me_t),
+        )
+
+    def send_dispatch(d, c):
+        @pl.when(d < own)
+        def _():
+            dispatch_out[d] = pick(me_t, d)
+            dispatch_copy(d).start()
+
+        @pl.when(d == own)
+        def _():
+            tokens[me_t, groups - 1, own_slots] = pick(me_t, own)
+
+        return c
+
+    def send_far(d):
+        for n, block in enumerate(far_blocks):
+            far_out[n, d] = pick(block, d)
+            far_copy(n, d).start()
+
+    rows = tokens.shape[2] // 2
 
     def expert(d):
         pieces = [tokens[j, d].astype(F32) for j in range(shards)]
@@ -693,76 +756,167 @@
     def combine(d, block):
         hidden[...] += dot(weight_high[d], block) + dot(weight_low[d], block)
 
-    def within(value):
-        return jnp.logical_and(value >= 0, value < groups)
+    def between(value, low, high):
+        return jnp.logical_and(value >= low, value < high)
 
     def take_done(d, c):
+        done_copy(d).wait_recv()
+        combine(d, done_in[d])
+        return c
+
+    def spread_wait(d):
+        spent(span(tokens, 2 * near, d), token_sems.at[1, d])
+
+    def pass_wait(d):
+        spent(span(tokens, near * near, d), token_sems.at[3, d])
+
+    def arrive_direct(i):
+        dispatch_copy(i).wait_recv()
+        spread_start(tokens, token_sems, i)
+
+    late = plane >= planes // 2
+
+    def feed_direct(i):
+        @pl.when(jnp.logical_and(jnp.logical_not(late), between(i, 2, own)))
+        def _():
+            arrive_direct(i)
+
+        @pl.when(i == 1)
+        def _():
+            spent(span(full, near * near, 0), early_sems.at[3, 0])
+            for t in range(shards):
+                partner_out[t] = pick(t, 0)
+            partner_copy().start()
+
+        @pl.when(jnp.logical_and(jnp.logical_not(late), i == 1))
+        def _():
+            arrive_direct(i)
+
+        @pl.when(jnp.logical_and(late, between(i, 1, own - 1)))
+        def _():
+            arrive_direct(i + 1)
+
+        @pl.when(between(i - 1, 1, far))
+        def _():
+            spread_wait(i - 1)
+            pass_start(tokens, token_sems, i - 1)
+
+    def launch_direct(i):
+        @pl.when(between(i, 1, own - ahead))
+        def _():
+            send_dispatch(i + ahead, 0)
+
+        @pl.when(between(i + ahead, far, own))
+        def _():
+            send_far(i + ahead)
+
+        @pl.when(i == 2)
+        def _():
+            for t in range(shards):
+                tokens[t, groups - 1] = pick(t, own)
+
+    def ready_direct(d):
         @pl.when(d == 0)
         def _():
-            combine(0, done_out[0, :capacity])
-
-        @pl.when(d > 0)
-        def _():
-            done_copy(d).wait_recv()
-            combine(d, done_in[d])
-
-        return c
-
-    lag = 6
-
-    def step(i, c):
-        @pl.when(within(i - 1))
-        def _():
-            for k in peers:
-                for dim in range(2):
-                    own_copy(dim, k, i - 1).wait_recv()
-            for dim in range(2):
-                for j in peers:
-                    for k in peers:
-                        pass_copy(dim, j, k, i - 1).start()
-
+            partner_copy().wait_recv()
+
+        @pl.when(between(d, 1, far))
+        def _():
+            pass_wait(d)
+
+        @pl.when(between(d, far, own))
+        def _():
+            spread_wait(d)
+            spent(far_out.at[:, d], far_recv.at[d])
+
+    def feed_grouped(i):
         @pl.when(i < groups)
         def _():
             def arrive(d, c):
-                @pl.when(d > 0)
+                @pl.when(d < own)
                 def _():
                     dispatch_copy(d).wait_recv()
 
                 return c
 
             lax.fori_loop(i * sources, (i + 1) * sources, arrive, 0)
-            for k in peers:
-                for dim in range(2):
-                    own_copy(dim, k, i).start()
-
-        @pl.when(i == 0)
-        def _():
-            if sources == 1:
-                lax.fori_loop(1, experts, send_dispatch, 0)
-            for load in loads[20:]:
-                load.wait()
-
-        @pl.when(within(i - 3))
+            spread_start(tokens, token_sems, i)
+
+        @pl.when(between(i - 1, 0, groups))
+        def _():
+            spread_wait(i - 1)
+            pass_start(tokens, token_sems, i - 1)
+
+        @pl.when(between(i, 1, groups - ahead))
+        def _():
+            launch(i + ahead)
+
+    def launch(group):
+        lax.fori_loop(group * sources, (group + 1) * sources, send_dispatch, 0)
+
+    def early_sent():
+        @pl.when(me_s < experts - 1)
+        def _():
+            for copy in rim_copies():
+                copy.wait_send()
+
+        @pl.when(core == 0)
+        def _():
+            pair_copy(column_count).wait_send()
+            spent(state_out, pair_send.at[0])
+
+        @pl.when(jnp.logical_and(core == 1, plane < planes - 1))
+        def _():
+            spent(chain_out, chain_send.at[0])
+
+        @pl.when(jnp.logical_and(core == 1, plane > 0))
+        def _():
+            spent(chain_in, relay_send.at[0])
+
+        sent(heads_bundle, 0)
+        if direct:
+            spent(span(full, 2 * near, 0), early_sems.at[0, 0])
+            spent(span(full, near * near, 0), early_sems.at[2, 0])
+
+    def tokens_sent(d):
+        spent(span(tokens, 2 * near, d), token_sems.at[0, d])
+
+    def passes_sent(d):
+        spent(span(tokens, near * near, d), token_sems.at[2, d])
+
+    steps = groups + 4
+
+    def step(i, c):
+        if direct:
+            feed_direct(i)
+        else:
+            feed_grouped(i)
+
+        @pl.when(between(i - 3, 0, groups))
         def _():
             forward(sums_bundle, i - 3)
 
-        @pl.when(within(i - 2))
-        def _():
-            for dim in range(2):
-                for j in peers:
-                    for k in peers:
-                        pass_copy(dim, j, k, i - 2).wait_recv()
+        @pl.when(between(i - 2, 0, groups))
+        def _():
+            if direct:
+                ready_direct(i - 2)
+            else:
+                pass_wait(i - 2)
             expert(i - 2)
 
-        @pl.when(within(i - 4))
-        def _():
+        if direct:
+            launch_direct(i)
+
+        @pl.when(between(i - 4, 0, groups))
+        def _():
+            settle(sums_bundle, i - 4)
             for dim in range(2):
                 done_out[i - 4, dim * rows : (dim + 1) * rows] = gathered(
                     sums_bundle, dim, i - 4
                 ).astype(BF16)
 
             def leave(d, c):
-                @pl.when(d > 0)
+                @pl.when(d < own)
                 def _():
                     done_copy(d).start()
 
@@ -770,58 +924,65 @@
 
             lax.fori_loop((i - 4) * sources, (i - 3) * sources, leave, 0)
 
-        @pl.when(within(i - lag))
+        @pl.when(between(i - lag, 0, groups))
         def _():
             lax.fori_loop((i - lag) * sources, (i - lag + 1) * sources, take_done, 0)
+            sent(sums_bundle, i - lag)
+
+        if direct:
+
+            @pl.when(between(i - 4, 1, own))
+            def _():
+                tokens_sent(i - 4)
+
+            @pl.when(between(i - 4, 1, far))
+            def _():
+                passes_sent(i - 4)
+        else:
+
+            @pl.when(between(i - 4, 0, groups))
+            def _():
+                tokens_sent(i - 4)
+                passes_sent(i - 4)
+
+        @pl.when(i == 3)
+        def _():
+            early_sent()
 
         return c
 
-    steps = groups + 4
-    if sources > 1:
-        lax.fori_loop(1, experts, send_dispatch, 0)
-    lax.fori_loop(0, steps, step, 0)
-    lax.fori_loop((steps - lag) * sources, experts, take_done, 0)
-    out_ref[...] = hidden[...].astype(BF16)
-
-    @pl.when(me_s < experts - 1)
-    def _():
-        for copy in rim_copies():
-            copy.wait_send()
-
-    @pl.when(core == 0)
-    def _():
-        for j in range(column_count + 1):
-            pair_copy(j).wait_send()
-
-    @pl.when(jnp.logical_and(core == 1, plane < planes - 1))
-    def _():
-        for j in range(column_count):
-            chain_copy(j).wait_send()
-
-    @pl.when(jnp.logical_and(core == 1, plane > 0))
-    def _():
-        for j in range(column_count):
-            relay_copy(j).wait_send()
-
-    sent(heads_bundle, 0)
-
-    def finish_sp(d, c):
-        dispatch_copy(d).wait_send()
-        done_copy(d).wait_send()
-        return c
-
-    lax.fori_loop(1, experts, finish_sp, 0)
-
-    def finish_group(d, c):
-        for dim in range(2):
-            for j in peers:
-                own_copy(dim, j, d).wait_send()
-                for k in peers:
-                    pass_copy(dim, j, k, d).wait_send()
-        sent(sums_bundle, d)
-        return c
-
-    lax.fori_loop(0, groups, finish_group, 0)
+    if direct:
+        spread_start(full, early_sems, 0)
+        for d in range(1, min(ahead + 1, own)):
+            send_dispatch(d, 0)
+        loaded(19, 22)
+        spent(span(full, 2 * near, 0), early_sems.at[1, 0])
+        pass_start(full, early_sems, 0)
+
+        @pl.when(late)
+        def _():
+            arrive_direct(1)
+    else:
+        for group in range(min(ahead + 1, groups)):
+            launch(group)
+        loaded(19, 22)
+    lax.fori_loop(1 if direct else 0, steps, step, 0)
+    lax.fori_loop((steps - lag) * sources, own, take_done, 0)
+    combine(own, done_out[groups - 1, own_slots])
+    out_v[...] = hidden[...].astype(BF16)
+    out_copy = pltpu.make_async_copy(out_v, out_ref, load_sem.at[0])
+    out_copy.start()
+    if direct:
+        spent(dispatch_out.at[pl.ds(1, own - 1)], dispatch_send.at[0])
+        partner_copy().wait_send()
+        if far < own:
+            spent(far_out.at[:, pl.ds(0, own - far)], far_send.at[0])
+    else:
+        spent(dispatch_out.at[pl.ds(0, own)], dispatch_send.at[0])
+    spent(done_in.at[pl.ds(0, own)], done_send.at[0])
+    for group in range(steps - lag, groups):
+        sent(sums_bundle, group)
+    out_copy.wait()
 
 
 def layer_call(side, experts, arrays):
@@ -845,6 +1006,8 @@
     vmem = pltpu.VMEM
     dma = pltpu.SemaphoreType.DMA
     scratch = [
+        vmem((RIM, wide_width + 2 * state), BF16),
+        vmem((RIM, narrow_width), BF16),
         vmem((RIM + length, wide_width + 2 * state), BF16),
         vmem((RIM + length, narrow_width), BF16),
         vmem((length, wide_width), BF16),
@@ -888,7 +1051,6 @@
         vmem((2, near, 1, length // 2, width), BF16),
         vmem((2, near, 1, length // 2, width), BF16),
         vmem((length, width), F32),
-        vmem((length, width), BF16),
         vmem((experts, capacity, length), BF16),
         vmem((experts, length, capacity), BF16),
         vmem((experts, length, capacity), BF16),
@@ -900,26 +1062,28 @@
         vmem((2, near, groups, rows // 2, width), BF16),
         vmem((groups, rows, width), BF16),
         vmem((experts, capacity, width), BF16),
-        dma((23,)),
+        vmem((shards, 1, length, width), BF16),
+        vmem((shards, capacity, width), BF16),
+        vmem((near * near, groups, rows, width), BF16),
+        vmem((length, width), BF16),
+        dma((22,)),
         dma((2,)),
         dma((2,)),
-        dma((column_count + 1,)),
-        dma((column_count + 1,)),
+        dma((2,)),
+        dma((2,)),
+        dma((1,)),
         dma((column_count,)),
+        dma((1,)),
         dma((column_count,)),
-        dma((column_count,)),
-        dma((column_count,)),
-        dma((2, 2, near, side, 1)),
-        dma((2, 2, near, 1)),
+        dma((4, 1)),
+        dma((4, 1)),
+        dma((2,)),
         dma((experts,)),
-        dma((experts,)),
-        dma((2, near, groups)),
-        dma((2, near, groups)),
-        dma((2, near, near, groups)),
-        dma((2, near, near, groups)),
-        dma((2, 2, near, side, groups)),
-        dma((2, 2, near, groups)),
-        dma((experts,)),
+        dma((1,)),
+        dma((groups,)),
+        dma((4, groups)),
+        dma((4, groups)),
+        dma((1,)),
         dma((experts,)),
     ]
     hbm = pl.BlockSpec(memory_space=pl.ANY)
@@ -931,7 +1095,7 @@
         functools.partial(layer_kernel, side, experts, capacity),
         out_shape=jax.ShapeDtypeStruct((length, width), BF16),
         in_specs=specs,
-        out_specs=pl.BlockSpec(memory_space=pltpu.VMEM),
+        out_specs=hbm,
         scratch_shapes=scratch,
         compiler_params=pltpu.CompilerParams(
             collective_id=0, has_side_effects=True, vmem_limit_bytes=60 * 1024 * 1024

time: 115 us -> 104 us (0.904); the launches traced: 113 us -> 104 us
  Pallas kernels: 111 us -> 102 us
    pallas_call x1, Pallas kernels: 111 us -> 102 us  [layer_call(): pl.pallas_call(functools.partial(layer_kernel, side, experts, capacity),...]
where the time goes in v2:
time: 104 us
  Pallas kernels  102 us (98%)
  local copies, waits for them, and re-layouts  1.67 us (2%)
    pallas_call x1, Pallas kernels, layer_call(): pl.pallas_call(functools.partial(layer_kernel, side, experts, capacity),...  102 us

profile of v2, /device:TPU:0, one launch (start us, length us, event | category | flops | bytes accessed | tf_op | source)
XLA Modules:
  0.0 103.7 jit_solution(2414231834069761935)
XLA Ops:
  0.0 102.0 %shard_map.235 = bf16[256,512]{1,0:T(8,128)(2,1)} custom-call(bf16[256,2048]{1,0:T(8,128)(2,1)} %resid_hbm.1, bf16[256,256]{1,0:T(8,128)(2,1)} %narrow_hbm.1, bf16[256,512]{1,0:T(8,128)(2,1)} %wide_hbm.1, bf16[256,512]{1,0:T(8,128)(2,1)} %key_hbm.1, bf16[256,512]{1,0:T(8,128)(2,1)} %query_hbm.1, bf16[256,256]{1,0:T(8,128)(2,1)} %narrow_gate_hbm.1, ...), custom_call_target="tpu_custom_call" | custom-call | tf_op jit(solution)/shard_map/pallas_call | solution.py:1094
  102.0 1.7 %copy.27 = bf16[256,512]{1,0:T(8,128)(2,1)} copy(bf16[256,512]{1,0:T(8,128)(2,1)} %shard_map.235) | data formatting | bytes 524288

commit v3 on v2

--- a/solution.py
+++ b/solution.py
@@ -12,7 +12,7 @@
 GROUPS = 4
 LANES = 128
 RIM = 16
-FAR_GROUPS = 2
+FAR_GROUPS = 4
 
 NORM_EPS = 1e-06
 CLAMP_LIMIT = 7.0
@@ -354,39 +354,44 @@
     for j, value in enumerate(factor_rows):
         factor_out[j : j + 1, :] = value
 
-    loaded(10, 16)
-
-    for j, (offset, size, _) in enumerate(columns):
-        source = wide_gate_v if j < wide_columns else narrow_gate_v
-        value = padded(source[:, offset : offset + size]).astype(F32)
-        gate_act[j] = value * sigmoid(value)
-
-    order = lax.broadcasted_iota(jnp.int32, (experts, length), 0)
-    mask = jnp.where(order < experts - 3, order + 3, order + 5 - experts)
-    mask = jnp.where(order == 0, 1, jnp.where(order == experts - 1, 0, mask))
-    named = mask ^ me_s
-    member = jnp.zeros((experts, length), F32)
-    weight_rows = jnp.zeros((experts, length), F32)
-    for k in range(routes_v.shape[0]):
-        hit = routes_v[k : k + 1, :] == named
-        member = jnp.where(hit, 1.0, member)
-        weight_rows = jnp.where(hit, route_weights_v[k : k + 1, :], weight_rows)
-    before = jnp.where(line < across, 1.0, 0.0).astype(BF16)
-    ranks = dot(member.astype(BF16), before)
-    ranks = jnp.where(member > 0.5, ranks, -1.0)
-    slots = lax.broadcasted_iota(jnp.int32, (capacity, length), 0).astype(F32)
-    slot_lanes = lax.broadcasted_iota(jnp.int32, (length, capacity), 1).astype(F32)
-    filler = [jnp.zeros((LANES - experts, length), F32)] if experts < LANES else []
-    rank_columns = jnp.transpose(jnp.concatenate([ranks] + filler, axis=0))
-    weight_columns = jnp.transpose(jnp.concatenate([weight_rows] + filler, axis=0))
-    for d in range(experts):
-        chooser[d] = jnp.where(slots == ranks[d : d + 1, :], 1.0, 0.0).astype(BF16)
-        weights = jnp.where(
-            slot_lanes == rank_columns[:, d : d + 1], weight_columns[:, d : d + 1], 0.0
-        )
-        rounded = weights.astype(BF16)
-        weight_high[d] = rounded
-        weight_low[d] = (weights - rounded.astype(F32)).astype(BF16)
+    def tables():
+        loaded(10, 16)
+
+        for j, (offset, size, _) in enumerate(columns):
+            source = wide_gate_v if j < wide_columns else narrow_gate_v
+            value = padded(source[:, offset : offset + size]).astype(F32)
+            gate_act[j] = value * sigmoid(value)
+
+        order = lax.broadcasted_iota(jnp.int32, (experts, length), 0)
+        mask = jnp.where(order < experts - 3, order + 3, order + 5 - experts)
+        mask = jnp.where(order == 0, 1, jnp.where(order == experts - 1, 0, mask))
+        named = mask ^ me_s
+        member = jnp.zeros((experts, length), F32)
+        weight_rows = jnp.zeros((experts, length), F32)
+        for k in range(routes_v.shape[0]):
+            hit = routes_v[k : k + 1, :] == named
+            member = jnp.where(hit, 1.0, member)
+            weight_rows = jnp.where(hit, route_weights_v[k : k + 1, :], weight_rows)
+        before = jnp.where(line < across, 1.0, 0.0).astype(BF16)
+        ranks = dot(member.astype(BF16), before)
+        ranks = jnp.where(member > 0.5, ranks, -1.0)
+        slots = lax.broadcasted_iota(jnp.int32, (capacity, length), 0).astype(F32)
+        slot_lanes = lax.broadcasted_iota(jnp.int32, (length, capacity), 1).astype(F32)
+        filler = [jnp.zeros((LANES - experts, length), F32)] if experts < LANES else []
+        rank_columns = jnp.transpose(jnp.concatenate([ranks] + filler, axis=0))
+        weight_columns = jnp.transpose(jnp.concatenate([weight_rows] + filler, axis=0))
+        for d in range(experts):
+            chooser[d] = jnp.where(slots == ranks[d : d + 1, :], 1.0, 0.0).astype(BF16)
+            weights = jnp.where(
+                slot_lanes == rank_columns[:, d : d + 1], weight_columns[:, d : d + 1], 0.0
+            )
+            rounded = weights.astype(BF16)
+            weight_high[d] = rounded
+            weight_low[d] = (weights - rounded.astype(F32)).astype(BF16)
+
+    @pl.when(plane > 0)
+    def _():
+        tables()
 
     @pl.when(me_s > 0)
     def _():
@@ -489,6 +494,10 @@
     for j in range(early, column_count):
         inside(j)
 
+    @pl.when(plane == 0)
+    def _():
+        tables()
+
     def carry_odd(j):
         chain_copy(j).wait_recv()
         relay_copy(j).start()
@@ -787,6 +796,7 @@
             for t in range(shards):
                 partner_out[t] = pick(t, 0)
             partner_copy().start()
+            send_dispatch(1 + ahead, 0)
 
         @pl.when(jnp.logical_and(jnp.logical_not(late), i == 1))
         def _():
@@ -802,13 +812,13 @@
             pass_start(tokens, token_sems, i - 1)
 
     def launch_direct(i):
-        @pl.when(between(i, 1, own - ahead))
+        @pl.when(between(i, 2, own - ahead))
         def _():
             send_dispatch(i + ahead, 0)
 
-        @pl.when(between(i + ahead, far, own))
-        def _():
-            send_far(i + ahead)
+        @pl.when(between(i + 1, far, own))
+        def _():
+            send_far(i + 1)
 
         @pl.when(i == 2)
         def _():

time: 104 us -> 99.9 us (0.961)
  Pallas kernels: 102 us -> 97.9 us
    pallas_call x1, Pallas kernels: 102 us -> 97.9 us  [layer_call(): pl.pallas_call(functools.partial(layer_kernel, side, experts, capacity),...]
where the time goes in v3:
time: 99.9 us; the launch traced here: 99.6 us
  Pallas kernels  97.9 us (98%)
  local copies, waits for them, and re-layouts  1.67 us (2%)
    pallas_call x1, Pallas kernels, layer_call(): pl.pallas_call(functools.partial(layer_kernel, side, experts, capacity),...  97.9 us

profile of v3, /device:TPU:0, one launch (start us, length us, event | category | flops | bytes accessed | tf_op | source)
XLA Modules:
  0.0 99.6 jit_solution(14126420990049831742)
XLA Ops:
  0.0 97.9 %shard_map.235 = bf16[256,512]{1,0:T(8,128)(2,1)} custom-call(bf16[256,2048]{1,0:T(8,128)(2,1)} %resid_hbm.1, bf16[256,256]{1,0:T(8,128)(2,1)} %narrow_hbm.1, bf16[256,512]{1,0:T(8,128)(2,1)} %wide_hbm.1, bf16[256,512]{1,0:T(8,128)(2,1)} %key_hbm.1, bf16[256,512]{1,0:T(8,128)(2,1)} %query_hbm.1, bf16[256,256]{1,0:T(8,128)(2,1)} %narrow_gate_hbm.1, ...), custom_call_target="tpu_custom_call" | custom-call | tf_op jit(solution)/shard_map/pallas_call | solution.py:1104
  98.0 1.7 %copy.27 = bf16[256,512]{1,0:T(8,128)(2,1)} copy(bf16[256,512]{1,0:T(8,128)(2,1)} %shard_map.235) | data formatting | bytes 524288

commit v4 on v3

--- a/solution.py
+++ b/solution.py
@@ -567,7 +567,7 @@
         _, _, mid, in2, sems = bundle
         peer = at(col, (row + k) % side) if dim == 0 else at((col + k) % side, row)
         return remote(
-            mid.at[dim, k - 1, d], in2.at[dim, k - 1, d], sems.at[3, d], sems.at[2, d], (me_s, peer)
+            mid.at[dim, k - 1, d], in2.at[dim, k - 1, d], sems.at[0, d], sems.at[2, d], (me_s, peer)
         )
 
     def scatter(bundle, d, produce):
@@ -610,8 +610,7 @@
 
     def sent(bundle, d):
         part, sems = bundle[0], bundle[4]
-        spent(part.at[d, pl.ds(0, near * side)], sems.at[0, d])
-        spent(part.at[d, pl.ds(0, near)], sems.at[3, d])
+        spent(part.at[d, pl.ds(0, near * side + near)], sems.at[0, d])
 
     def project(block):
         lanes = pl.ds(pl.multiple_of(block * width, LANES), width)
@@ -1085,14 +1084,14 @@
         dma((column_count,)),
         dma((1,)),
         dma((column_count,)),
-        dma((4, 1)),
+        dma((3, 1)),
         dma((4, 1)),
         dma((2,)),
         dma((experts,)),
         dma((1,)),
         dma((groups,)),
         dma((4, groups)),
-        dma((4, groups)),
+        dma((3, groups)),
         dma((1,)),
         dma((experts,)),
     ]

time: 99.9 us -> 99.8 us (level)
  no operation moved by 1% of the time
where the time goes in v4:
time: 99.8 us; the launch traced here: 99.5 us
  Pallas kernels  97.9 us (98%)
  local copies, waits for them, and re-layouts  1.67 us (2%)
    pallas_call x1, Pallas kernels, layer_call(): pl.pallas_call(functools.partial(layer_kernel, side, experts, capacity),...  97.9 us

profile of v4, /device:TPU:0, one launch (start us, length us, event | category | flops | bytes accessed | tf_op | source)
XLA Modules:
  0.0 99.5 jit_solution(15701925733572442295)
XLA Ops:
  0.0 97.9 %shard_map.235 = bf16[256,512]{1,0:T(8,128)(2,1)} custom-call(bf16[256,2048]{1,0:T(8,128)(2,1)} %resid_hbm.1, bf16[256,256]{1,0:T(8,128)(2,1)} %narrow_hbm.1, bf16[256,512]{1,0:T(8,128)(2,1)} %wide_hbm.1, bf16[256,512]{1,0:T(8,128)(2,1)} %key_hbm.1, bf16[256,512]{1,0:T(8,128)(2,1)} %query_hbm.1, bf16[256,256]{1,0:T(8,128)(2,1)} %narrow_gate_hbm.1, ...), custom_call_target="tpu_custom_call" | custom-call | tf_op jit(solution)/shard_map/pallas_call | solution.py:1103
  97.9 1.7 %copy.27 = bf16[256,512]{1,0:T(8,128)(2,1)} copy(bf16[256,512]{1,0:T(8,128)(2,1)} %shard_map.235) | data formatting | bytes 524288
